TPU v7x, 256 devices: a whole 4x4x8 slice. The times are simulated.
256 devices in a mesh: sp: 64 (over z, y, core), tp: 4 (over x).
Axes of the slice: x: 4, y: 4, z: 8, core: 2. Of those that a mesh axis runs over, the one named last changes fastest.
Arguments:
- stream: bfloat16 [8192, 2048], P('sp', 'tp'), may hold values from -40 to 40
- queries: bfloat16 [8192, 1024], P('sp', 'tp'), may hold values from -6 to 6
- keys: bfloat16 [8192, 1024], P('sp', 'tp'), may hold values from -6 to 6
- values: bfloat16 [8192, 2048], P('sp', 'tp'), may hold values from -25 to 25
- out_gate: bfloat16 [8192, 2048], P('sp', 'tp'), may hold values from -8 to 8
- input_gate: float32 [8192, 8], P('sp', 'tp'), may hold values from -9 to 350
- forget_gate: float32 [8192, 8], P('sp', 'tp'), may hold values from -4 to 20
- head_gain: float32 [2048], P('tp'), may hold values from 0.1 to 1.9
- w_out: bfloat16 [2048, 2048], P('tp'), may hold values from -0.125 to 0.125
- ffn_gain: float32 [2048], replicated, may hold values from 0.1 to 1.9
- w_gate: bfloat16 [2048, 5632], P('sp', 'tp'), may hold values from -0.125 to 0.125
- w_up: bfloat16 [2048, 5632], P('sp', 'tp'), may hold values from -0.125 to 0.125
- w_down: bfloat16 [5632, 2048], P('tp', 'sp'), may hold values from -0.078125 to 0.078125
Outputs:
- mixed: bfloat16 [8192, 2048], P('sp', 'tp')
All inputs are finite; a program needn't handle non-finite values.
Results may differ from a plain program's by a relative error of at most 0.0095.
Values may be sent and summed in bfloat16 or wider, within the bound.
A program may use at most 128 MiB of HBM per device.

v0:
```python
import jax
import jax.numpy as jnp
from jax import lax
from jax.sharding import Mesh
from jax.sharding import PartitionSpec as P

D = 2048
DQK = 128
DV = 256
BLOCK = 64
VALS = 2048
SP = ("sp_0", "sp_1", "sp_2")


precise = lax.Precision.HIGHEST
norm_eps = 1e-06
very_low = -1e30


def gather_turned(arrays, axis, dims):
    turned = [jnp.moveaxis(a, dim, 0) for a, dim in zip(arrays, dims)]
    both = jnp.concatenate([t.reshape(len(t), -1) for t in turned], axis=1)
    result, at, gathered = (lax.all_gather(both, axis, axis=0, tiled=True), 0, [])
    for t, dim in zip(turned, dims):
        slab = result[:, at : at + t[0].size].reshape(-1, *t.shape[1:])
        gathered.append(jnp.moveaxis(slab, 0, dim))
        at += t[0].size
    return tuple(gathered)


def nothing_yet(x, identity):
    return jax.tree.map(
        lambda a, e: jnp.broadcast_to(jnp.asarray(e, a.dtype), a.shape), x, identity
    )


def all_in_one(x, axis):
    leaves = jax.tree.leaves(x)
    order = sorted(range(len(leaves)), key=lambda k: -leaves[k].size)
    width = (1, *leaves[order[0]].shape)[-1]
    lines = [
        jnp.pad(leaves[k].reshape(-1), (0, -leaves[k].size % width)).reshape(-1, width)
        for k in order
    ]
    both, at, found = (lax.all_gather(jnp.concatenate(lines), axis), 0, {})
    for k, line in zip(order, lines):
        slab = both[:, at : at + len(line)].reshape(len(both), -1)
        found[k] = slab[:, : leaves[k].size].reshape(-1, *leaves[k].shape)
        at += len(line)
    numbers = iter(range(len(leaves)))
    return jax.tree.map(lambda _: found[next(numbers)], x)


def entering(x, axes, combine, identity):
    before = start = nothing_yet(x, identity)
    subtotal = x
    for axis in reversed(axes):
        peers, mine = (lax.axis_size(axis), lax.axis_index(axis))
        pieces = all_in_one(subtotal, axis)
        inside, subtotal = (start, start)
        for k in range(peers):
            passed = k < mine
            subtotal = combine(subtotal, jax.tree.map(lambda part: part[k], pieces))
            inside = jax.tree.map(lambda new, old: jnp.where(passed, new, old), subtotal, inside)
        before = combine(inside, before)
    return before


def copy_for_each(x, axis):
    peers = lax.axis_size(axis)
    return lax.all_to_all(jnp.broadcast_to(x[None], (peers, *x.shape)), axis, 0, 0, tiled=True)


def over_copies(x, axis):
    everything = copy_for_each(x, axis)
    return jnp.sum(everything, axis=0)


def cut_along(x, dim, peers):
    shape = x.shape
    parts = x.reshape(*shape[:dim], peers, shape[dim] // peers, *shape[dim + 1 :])
    return jnp.moveaxis(parts, dim, 0)


def summed_on_arrival(x, axis, dim):
    parts = cut_along(x, dim, lax.axis_size(axis))
    arrived = lax.all_to_all(parts, axis, split_axis=0, concat_axis=0, tiled=True)
    return arrived.astype(jnp.float32).sum(axis=0)


def in_order(parts, dim):
    shape = list(parts.shape[1:])
    shape[dim] *= parts.shape[0]
    return jnp.moveaxis(parts, 0, dim).reshape(shape)


def gathered_copies(x, axis, dim):
    parts = copy_for_each(x, axis)
    return in_order(parts, dim)


def block_summary(key_blk, value_blk, input_blk, decay_sum):
    decay_total = decay_sum[..., -1]
    log_weight = decay_total[..., None] - decay_sum + input_blk
    weight_peak = jnp.max(log_weight, axis=-1)
    weights = jnp.exp(log_weight - weight_peak[..., None])
    state_mat = jnp.einsum(
        "...ld,...le->...de", weights[..., None] * key_blk, value_blk, precision=precise
    )
    state_vec = jnp.einsum("...l,...ld->...d", weights, key_blk, precision=precise)
    return (state_mat, state_vec, weight_peak, decay_total)


def combine(earlier, later):
    ceiling = jnp.maximum(later[3] + earlier[2], later[2])
    former = jnp.exp(later[3] + earlier[2] - ceiling)
    latter = jnp.exp(later[2] - ceiling)
    return (
        former[..., None, None] * earlier[0] + latter[..., None, None] * later[0],
        former[..., None] * earlier[1] + latter[..., None] * later[1],
        ceiling,
        earlier[3] + later[3],
    )


def block_output(
    query_blk, key_blk, value_blk, input_blk, decay_sum, state_mat, state_vec, state_peak
):
    block_len = query_blk.shape[-2]
    causal = jnp.tril(jnp.ones((block_len, block_len), jnp.bool_))
    log_pair = jnp.where(
        causal,
        decay_sum[..., :, None] - decay_sum[..., None, :] + input_blk[..., None, :],
        -jnp.inf,
    )
    log_carry = decay_sum + state_peak[..., None]
    row_peak = jnp.maximum(log_carry, jnp.max(log_pair, axis=-1))
    scores = jnp.einsum("...ld,...sd->...ls", query_blk, key_blk, precision=precise) * jnp.exp(
        log_pair - row_peak[..., None]
    )
    carried = jnp.exp(log_carry - row_peak)
    numer = jnp.einsum("...ls,...se->...le", scores, value_blk, precision=precise) + carried[
        ..., None
    ] * jnp.einsum("...ld,...de->...le", query_blk, state_mat, precision=precise)
    normer = jnp.sum(scores, axis=-1) + carried * jnp.einsum(
        "...ld,...d->...l", query_blk, state_vec, precision=precise
    )
    denom = jnp.maximum(jnp.abs(normer), jnp.exp(-row_peak))
    return numer / denom[..., None]


def local(
    stream,
    queries,
    keys,
    values,
    out_gate,
    input_gate,
    forget_gate,
    head_gain,
    w_out,
    ffn_gain,
    w_gate,
    w_up,
    w_down,
):
    gate_full, up_full, down_full = gather_turned((w_gate, w_up, w_down), SP, (0, 0, 1))
    count_of_rows = stream.shape[0]
    head_count = input_gate.shape[1]
    blocks = count_of_rows // BLOCK

    def to_blocks(array, col_width):
        return (
            array.astype(jnp.float32)
            .reshape(blocks, BLOCK, head_count, col_width)
            .transpose(2, 0, 1, 3)
        )

    query_blk = to_blocks(queries, DQK) * DQK ** (-0.5)
    key_blk = to_blocks(keys, DQK)
    value_blk = to_blocks(values, DV)
    input_blk = input_gate.reshape(blocks, BLOCK, head_count).transpose(2, 0, 1)
    decay_sum = jnp.cumsum(
        jax.nn.log_sigmoid(forget_gate).reshape(blocks, BLOCK, head_count).transpose(2, 0, 1),
        axis=-1,
    )
    summary = block_summary(key_blk, value_blk, input_blk, decay_sum)
    identity = (
        jnp.zeros((head_count, DQK, DV), jnp.float32),
        jnp.zeros((head_count, DQK), jnp.float32),
        jnp.full((head_count,), very_low, jnp.float32),
        jnp.zeros((head_count,), jnp.float32),
    )

    def advance(carry, piece):
        return (combine(carry, piece), carry)

    local_total, prefix = lax.scan(
        advance, identity, jax.tree.map(lambda array: jnp.moveaxis(array, 1, 0), summary)
    )
    carry_in = entering(local_total, SP, combine, identity)
    start = combine(
        jax.tree.map(lambda array: array[:, None], carry_in),
        jax.tree.map(lambda array: jnp.moveaxis(array, 0, 1), prefix),
    )
    mixed_heads = block_output(
        query_blk, key_blk, value_blk, input_blk, decay_sum, start[0], start[1], start[2]
    )
    head_rows = mixed_heads.transpose(1, 2, 0, 3).reshape(count_of_rows, head_count, DV)
    local_sq = jnp.sum(head_rows * head_rows, axis=(1, 2))
    total_sq = over_copies(local_sq, "tp")
    row_scale = lax.rsqrt(total_sq / VALS + norm_eps)
    gated = (
        head_rows
        * row_scale[:, None, None]
        * head_gain.reshape(head_count, DV)
        * jax.nn.sigmoid(out_gate.astype(jnp.float32).reshape(count_of_rows, head_count, DV))
    )
    heads_out = gated.reshape(count_of_rows, head_count * DV).astype(jnp.bfloat16)
    partial_value = jnp.dot(heads_out, w_out, preferred_element_type=jnp.float32)
    col_width = stream.shape[1]
    col_start = lax.axis_index("tp") * col_width
    mixer_own = summed_on_arrival(partial_value.astype(jnp.bfloat16), "tp", 1)
    resid_own = (stream.astype(jnp.float32) + mixer_own).astype(jnp.bfloat16)
    resid_f = resid_own.astype(jnp.float32)
    square_total = over_copies(jnp.sum(resid_f * resid_f, axis=-1), "tp")
    gain_own = lax.dynamic_slice_in_dim(ffn_gain, col_start, col_width)
    normed_own = (resid_f * lax.rsqrt(square_total / D + norm_eps)[:, None] * gain_own).astype(
        jnp.bfloat16
    )
    normed = gathered_copies(normed_own, "tp", 1)
    gate_act = jnp.dot(normed, gate_full, preferred_element_type=jnp.float32)
    up_act = jnp.dot(normed, up_full, preferred_element_type=jnp.float32)
    hidden = (jax.nn.silu(gate_act) * up_act).astype(jnp.bfloat16)
    term = jnp.dot(hidden, down_full, preferred_element_type=jnp.float32)
    down_own = summed_on_arrival(term.astype(jnp.bfloat16), "tp", 1)
    return (resid_own.astype(jnp.float32) + down_own).astype(jnp.bfloat16)


def solution(mesh):
    split = Mesh(mesh.devices.reshape(8, 4, 2, mesh.shape["tp"]), ("sp_0", "sp_1", "sp_2", "tp"))
    in_specs = (
        P(SP, "tp"),
        P(SP, "tp"),
        P(SP, "tp"),
        P(SP, "tp"),
        P(SP, "tp"),
        P(SP, "tp"),
        P(SP, "tp"),
        P("tp"),
        P("tp", None),
        P(),
        P(SP, "tp"),
        P(SP, "tp"),
        P("tp", SP),
    )
    out_specs = P(SP, "tp")
    return jax.shard_map(local, mesh=split, in_specs=in_specs, out_specs=out_specs, check_vma=False)
```

profile of v0, /device:TPU:1, one launch (start us, length us, event | category | flops | bytes accessed | tf_op | source)
XLA Modules:
  0.0 230.6 jit_solution(16289289867176333970)
XLA Ops:
  6.6 0.8 fusion.83
  9.1 0.9 reshape.3322
  10.0 1.0 reshape.3325
  11.8 2.1 while.25
  14.5 5.0 %all-gather.3 = f32[2,259,256]{2,1,0:T(8,128)S(1)} all-gather(f32[1,259,256]{2,1,0:T(8,128)S(1)} %maximum_bitcast_fusion), channel_id=2, replica_groups=mesh['sp_0'=8,'sp_1'=4,'sp_2'=2,'tp'=4] {'sp_2'}, dimensions={0}, use_global_device_ids=true | all-gather | bytes 795648 | tf_op jit(solution)/shard_map/all_gather | solution.py:45
  21.5 25.7 %all-gather.12.cloned.1.call-done = f32[4,259,256]{2,1,0:T(8,128)} async-done(((f32[1,259,256]{2,1,0:T(8,128)}), f32[4,259,256]{2,1,0:T(8,128)}) %all-gather.12.cloned.1.call-update) | async-done | bytes 1060880 | tf_op jit(solution)/shard_map/all_gather | solution.py:45
  47.2 0.8 fusion.155
  48.9 1.5 fusion.43
  55.7 1.4 fusion.153
  57.0 2.0 fusion.154
  59.0 33.0 %all-gather.14.cloned.1.call-done = f32[8,259,256]{2,1,0:T(8,128)} async-done(((f32[1,259,256]{2,1,0:T(8,128)}), f32[8,259,256]{2,1,0:T(8,128)}) %all-gather.14.cloned.1.call-update) | async-done | bytes 2121744 | tf_op jit(solution)/shard_map/all_gather | solution.py:45
  92.0 0.9 fusion.152
  94.5 1.2 subtract_exponential_fusion.23
  96.3 1.3 fusion.85
  97.5 1.3 copy.70
  98.8 1.3 add_maximum_fusion.1
  100.1 1.3 copy.72
  105.1 1.0 subtract_exponential_fusion.21
  106.1 0.9 multiply_add_fusion.1
  107.8 1.2 fusion.55
  109.0 1.2 fusion.159
  111.5 1.6 fusion.151
  115.6 3.7 %all-to-all-start = ((f32[4,1,128]{2,1,0:T(1,128)}), f32[4,1,128]{2,1,0:T(1,128)S(1)}, u32[]{:S(2)}, u32[]{:S(2)}) async-start(f32[4,1,128]{2,1,0:T(1,128)} %broadcast_in_dim.49), calls=%async_computation | async-start | bytes 4096 | tf_op jit(solution)/shard_map/all_to_all | solution.py:71
  119.5 3.8 %all-to-all-done = f32[4,1,128]{2,1,0:T(1,128)S(1)} async-done(((f32[4,1,128]{2,1,0:T(1,128)}), f32[4,1,128]{2,1,0:T(1,128)S(1)}, u32[]{:S(2)}, u32[]{:S(2)}) %all-to-all-start) | async-done | bytes 2080 | tf_op jit(solution)/shard_map/all_to_all | solution.py:71
  124.0 9.3 %all_to_all.27 = bf16[4,128,512]{2,1,0:T(8,128)(2,1)S(1)} all-to-all(bf16[4,128,512]{2,1,0:T(8,128)(2,1)S(1)} %bitcast.624), channel_id=1, replica_groups=mesh['sp_0'=8,'sp_1'=4,'sp_2'=2,'tp'=4] {'tp'}, dimensions={0} | all-to-all | bytes 1048576 | tf_op jit(solution)/shard_map/all_to_all | solution.py:87
  134.1 3.2 %all-to-all-start.2 = ((f32[4,1,128]{2,1,0:T(1,128)}), f32[4,1,128]{2,1,0:T(1,128)S(1)}, u32[]{:S(2)}, u32[]{:S(2)}) async-start(f32[4,1,128]{2,1,0:T(1,128)} %broadcast_in_dim.50), calls=%async_computation.2 | async-start | bytes 4096 | tf_op jit(solution)/shard_map/all_to_all | solution.py:71
  138.1 3.3 %all-to-all-done.2 = f32[4,1,128]{2,1,0:T(1,128)S(1)} async-done(((f32[4,1,128]{2,1,0:T(1,128)}), f32[4,1,128]{2,1,0:T(1,128)S(1)}, u32[]{:S(2)}, u32[]{:S(2)}) %all-to-all-start.2) | async-done | bytes 2080 | tf_op jit(solution)/shard_map/all_to_all | solution.py:71
  141.7 9.3 %all_to_all.28 = bf16[4,128,512]{1,2,0:T(8,128)(2,1)S(1)} all-to-all(bf16[4,128,512]{1,2,0:T(8,128)(2,1)S(1)} %broadcast_in_dim.51), channel_id=1, replica_groups=mesh['sp_0'=8,'sp_1'=4,'sp_2'=2,'tp'=4] {'tp'}, dimensions={0} | all-to-all | bytes 1048576 | tf_op jit(solution)/shard_map/all_to_all | solution.py:71
  151.0 47.5 %all-gather.10.cloned.1.call-done = bf16[2048,4224]{1,0:T(8,128)(2,1)} async-done(((bf16[32,4224]{1,0:T(8,128)(2,1)}), bf16[2048,4224]{1,0:T(8,128)(2,1)}) %all-gather.10.cloned.1.call-update) | async-done | bytes 17301520 | tf_op jit(solution)/shard_map/all_gather | solution.py:23
  198.5 4.5 %fusion.15 = f32[128,1408]{1,0:T(8,128)} fusion(bf16[128,2048]{0,1:T(8,128)(2,1)S(1)} %bitcast.641, bf16[2048,4224]{1,0:T(8,128)(2,1)} %all-gather.10.cloned.1.call-done), kind=kOutput, calls=%fused_computation.26 | convolution fusion | flops 738197504 | bytes 7012352 | tf_op jit(solution)/shard_map/dot_general | solution.py:232
  203.0 7.4 %fusion.20 = bf16[128,2048]{1,0:T(8,128)(2,1)S(1)} fusion(bf16[2048,4224]{1,0:T(8,128)(2,1)} %all-gather.10.cloned.1.call-done, bf16[128,2048]{0,1:T(8,128)(2,1)S(1)} %bitcast.642, f32[128,1408]{1,0:T(8,128)} %fusion.15), kind=kOutput, calls=%fused_computation.29 | convolution fusion | flops 1477738496 | bytes 13303808 | tf_op jit(solution)/shard_map/dot_general | solution.py:235
  210.5 12.8 %all_to_all.29 = bf16[4,128,512]{2,1,0:T(8,128)(2,1)S(1)} all-to-all(bf16[4,128,512]{2,1,0:T(8,128)(2,1)S(1)} %bitcast.625), channel_id=1, replica_groups=mesh['sp_0'=8,'sp_1'=4,'sp_2'=2,'tp'=4] {'tp'}, dimensions={0} | all-to-all | bytes 1048576 | tf_op jit(solution)/shard_map/all_to_all | solution.py:87
  (264 shorter events, 25.9 us)
Async XLA Ops:
  6.5 116.8 %copy-start = (bf16[512,2048]{1,0:T(8,128)(2,1)S(1)}, bf16[512,2048]{1,0:T(8,128)(2,1)}, u32[]{:S(2)}) copy-start(bf16[512,2048]{1,0:T(8,128)(2,1)} %param.23) | copy-start | bytes 6291460
  6.5 40.7 %all-gather.12.cloned.1.call-start = ((), (), s32[]{:S(2)}) async-start(), calls=%async_computation.6 | async-start | bytes 1351680 | tf_op jit(solution)/shard_map/all_gather | solution.py:45
  8.0 46.2 %copy-start.5 = (f32[2,2,64]{2,1,0:T(2,128)}, f32[2,2,64]{2,1,0:T(2,128)S(1)}, u32[]{:S(2)}) copy-start(f32[2,2,64]{2,1,0:T(2,128)S(1)} %reduce_window_sum.13) | copy-start | bytes 3076
  8.9 45.3 %copy-start.13 = (f32[2,64,2]{1,0,2:T(2,128)}, f32[2,64,2]{1,0,2:T(2,128)S(1)}, u32[]{:S(2)}) copy-start(f32[2,64,2]{1,0,2:T(2,128)S(1)} %reshape.3324) | copy-start | bytes 3076
  14.0 5.6 %copy-start.57 = (f32[2,2]{1,0:T(2,128)}, f32[2,2]{1,0:T(2,128)S(1)}, u32[]{:S(2)}) copy-start(f32[2,2]{1,0:T(2,128)S(1)} %get-tuple-element.79) | copy-start | bytes 52
  14.0 6.0 %copy-start.16 = (f32[2,2]{1,0:T(2,128)}, f32[2,2]{1,0:T(2,128)S(1)}, u32[]{:S(2)}) copy-start(f32[2,2]{1,0:T(2,128)S(1)} %get-tuple-element.84) | copy-start | bytes 52
  19.5 33.0 %copy-start.7 = (bf16[1408,32]{0,1:T(8,128)(2,1)S(1)}, bf16[1408,32]{0,1:T(8,128)(2,1)}, u32[]{:S(2)}) copy-start(bf16[1408,32]{0,1:T(8,128)(2,1)} %param.27) | copy-start | bytes 270340
  19.5 33.1 %copy-start.8 = (bf16[32,1408]{1,0:T(8,128)(2,1)S(1)}, bf16[32,1408]{1,0:T(8,128)(2,1)}, u32[]{:S(2)}) copy-start(bf16[32,1408]{1,0:T(8,128)(2,1)} %param.26) | copy-start | bytes 270340
  19.5 33.1 %copy-start.9 = (bf16[32,1408]{1,0:T(8,128)(2,1)S(1)}, bf16[32,1408]{1,0:T(8,128)(2,1)}, u32[]{:S(2)}) copy-start(bf16[32,1408]{1,0:T(8,128)(2,1)} %param.25) | copy-start | bytes 270340
  19.7 28.4 %copy-start.50 = (f32[2]{0:T(128)}, f32[2]{0:T(128)S(1)}, u32[]{:S(2)}) copy-start(f32[2]{0:T(128)S(1)} %get-tuple-element.309) | copy-start | bytes 28
  20.4 33.1 %copy-start.10 = (bf16[128,256]{1,0:T(8,128)(2,1)S(1)}, bf16[128,256]{1,0:T(8,128)(2,1)}, u32[]{:S(2)}) copy-start(bf16[128,256]{1,0:T(8,128)(2,1)} %param.16) | copy-start | bytes 196612
  21.5 70.5 %all-gather.14.cloned.1.call-start = ((), (), s32[]{:S(2)}) async-start(), calls=%async_computation.7 | async-start | bytes 2433024 | tf_op jit(solution)/shard_map/all_gather | solution.py:45
  48.1 6.8 %copy-start.15 = (f32[4,1,256]{2,0,1:T(4,128)}, f32[4,1,256]{2,0,1:T(4,128)S(1)}, u32[]{:S(2)}) copy-start(f32[4,1,256]{2,0,1:T(4,128)S(1)} %copy.153) | copy-start | bytes 12292
  48.1 6.8 %copy-start.27 = (f32[2]{0:T(128)}, f32[2]{0:T(128)S(1)}, u32[]{:S(2)}) copy-start(f32[2]{0:T(128)S(1)} %get-tuple-element.241) | copy-start | bytes 28
  48.2 6.8 %copy-start.23 = (f32[2]{0:T(128)}, f32[2]{0:T(128)S(1)}, u32[]{:S(2)}) copy-start(f32[2]{0:T(128)S(1)} %get-tuple-element.243) | copy-start | bytes 28
  48.2 6.8 %copy-start.34 = (f32[2]{0:T(128)}, f32[2]{0:T(128)S(1)}, u32[]{:S(2)}) copy-start(f32[2]{0:T(128)S(1)} %get-tuple-element.242) | copy-start | bytes 28
  48.2 6.8 %copy-start.36 = (f32[2]{0:T(128)}, f32[2]{0:T(128)S(1)}, u32[]{:S(2)}) copy-start(f32[2]{0:T(128)S(1)} %get-tuple-element.305) | copy-start | bytes 28
  48.2 6.7 %copy-start.28 = (f32[2]{0:T(128)}, f32[2]{0:T(128)S(1)}, u32[]{:S(2)}) copy-start(f32[2]{0:T(128)S(1)} %get-tuple-element.245) | copy-start | bytes 28
  48.2 6.7 %copy-start.38 = (f32[2]{0:T(128)}, f32[2]{0:T(128)S(1)}, u32[]{:S(2)}) copy-start(f32[2]{0:T(128)S(1)} %get-tuple-element.244) | copy-start | bytes 28
  48.3 6.7 %copy-start.32 = (f32[2]{0:T(128)}, f32[2]{0:T(128)S(1)}, u32[]{:S(2)}) copy-start(f32[2]{0:T(128)S(1)} %get-tuple-element.247) | copy-start | bytes 28
  48.3 6.7 %copy-start.33 = (f32[2]{0:T(128)}, f32[2]{0:T(128)S(1)}, u32[]{:S(2)}) copy-start(f32[2]{0:T(128)S(1)} %get-tuple-element.308) | copy-start | bytes 28
  52.5 146.0 %all-gather.10.cloned.1.call-start = ((), (), s32[]{:S(2)}) async-start(), calls=%async_computation.5 | async-start | bytes 17571840 | tf_op jit(solution)/shard_map/all_gather | solution.py:23
  55.6 47.2 %copy-start.6 = (f32[2,2,64]{2,1,0:T(2,128)S(1)}, f32[2,2,64]{2,1,0:T(2,128)}, u32[]{:S(2)}) copy-start(f32[2,2,64]{2,1,0:T(2,128)} %copy-done.5) | copy-start | bytes 3076
  55.7 53.3 %copy-start.14 = (f32[2,64,2]{1,0,2:T(2,128)S(1)}, f32[2,64,2]{1,0,2:T(2,128)}, u32[]{:S(2)}) copy-start(f32[2,64,2]{1,0,2:T(2,128)} %copy-done.13) | copy-start | bytes 3076
  93.6 3.9 %copy-start.24 = (f32[2]{0:T(128)}, f32[2]{0:T(128)S(1)}, u32[]{:S(2)}) copy-start(f32[2]{0:T(128)S(1)} %get-tuple-element.235) | copy-start | bytes 28
  93.6 3.9 %copy-start.25 = (f32[2]{0:T(128)}, f32[2]{0:T(128)S(1)}, u32[]{:S(2)}) copy-start(f32[2]{0:T(128)S(1)} %get-tuple-element.236) | copy-start | bytes 28
  93.6 3.9 %copy-start.26 = (f32[2]{0:T(128)}, f32[2]{0:T(128)S(1)}, u32[]{:S(2)}) copy-start(f32[2]{0:T(128)S(1)} %get-tuple-element.237) | copy-start | bytes 28
  114.2 9.2 %copy-start.64 = (bf16[128,512]{1,0:T(8,128)(2,1)S(1)}, bf16[128,512]{1,0:T(8,128)(2,1)}, u32[]{:S(2)}) copy-start(bf16[128,512]{1,0:T(8,128)(2,1)} %param.19) | copy-start | bytes 393220
  114.2 9.2 %copy-start.65 = (f32[512]{0:T(512)S(1)}, f32[512]{0:T(512)}, u32[]{:S(2)}) copy-start(f32[512]{0:T(512)} %param.22) | copy-start | bytes 6148
  115.6 7.7 %all-to-all-start = ((f32[4,1,128]{2,1,0:T(1,128)}), f32[4,1,128]{2,1,0:T(1,128)S(1)}, u32[]{:S(2)}, u32[]{:S(2)}) async-start(f32[4,1,128]{2,1,0:T(1,128)} %broadcast_in_dim.49), calls=%async_computation | async-start | bytes 4096 | tf_op jit(solution)/shard_map/all_to_all | solution.py:71
  123.9 9.5 %copy-start.4 = (bf16[128,512]{1,0:T(8,128)(2,1)S(1)}, bf16[128,512]{1,0:T(8,128)(2,1)}, u32[]{:S(2)}) copy-start(bf16[128,512]{1,0:T(8,128)(2,1)} %param.15) | copy-start | bytes 393220
  134.1 7.3 %all-to-all-start.2 = ((f32[4,1,128]{2,1,0:T(1,128)}), f32[4,1,128]{2,1,0:T(1,128)S(1)}, u32[]{:S(2)}, u32[]{:S(2)}) async-start(f32[4,1,128]{2,1,0:T(1,128)} %broadcast_in_dim.50), calls=%async_computation.2 | async-start | bytes 4096 | tf_op jit(solution)/shard_map/all_to_all | solution.py:71
  (39 other events, 61.0 us)
Sparse Core Ops, SparseCore 0:
  21.6 25.6 all-gather.11
  52.7 39.3 all-gather.13
  94.7 103.7 all-gather.9
where the time goes:
time: 232 us; the launch traced here: 231 us
  waiting for transfers between devices  113 us (49%)
  blocking collectives  36.5 us (16%)
  other arithmetic  22.5 us (10%)
  local copies, waits for them, and re-layouts  20.5 us (9%)
  matrix products  16.5 us (7%)
  between operations  14.3 us (6%)
  starting transfers between devices  6.98 us (3%)
    all_gather x2, waiting for transfers between devices, all_in_one(): both, at, found = (lax.all_gather(jnp.concatenate(lines), axis), 0, {})  58.7 us
    all_gather x1, waiting for transfers between devices, gather_turned(): lax.all_gather(both, axis, axis=0, tiled=True)  47.5 us
    all_to_all x2, blocking collectives, summed_on_arrival(): lax.all_to_all(parts, axis, split_axis=0, concat_axis=0, tiled=True)  22.1 us
    all_to_all x1, blocking collectives, copy_for_each(): lax.all_to_all(jnp.broadcast_to(x[None], (peers, *x.shape)), axis, 0, 0,...  9.34 us
    dot_general x1, matrix products, local(): term = jnp.dot(hidden, down_full, preferred_element_type=jnp.float32)  7.41 us
    all_to_all x2, waiting for transfers between devices, copy_for_each(): lax.all_to_all(jnp.broadcast_to(x[None], (peers, *x.shape)), axis, 0, 0,...  7.08 us
    all_to_all x2, starting transfers between devices, copy_for_each(): lax.all_to_all(jnp.broadcast_to(x[None], (peers, *x.shape)), axis, 0, 0,...  6.89 us
    slice x6, local copies, waits for them, and re-layouts, entering(): subtotal = combine(subtotal, jax.tree.map(lambda part: part[k], pieces))  6.41 us
  transfers between devices with their start and end apart: 5, of which 5 were waited for; matrix products, arithmetic and copies ran while one was open for 14% of the time, Pallas kernels for 0%

commit v1 on v0

v1 whole, which is shorter than its diff:
```python
import functools

import jax
import jax.numpy as jnp
from jax import lax
from jax.experimental import pallas as pl
from jax.experimental.pallas import tpu as pltpu
from jax.sharding import PartitionSpec as P

D = 2048
DQK = 128
DV = 256
VALS = 2048
FFT = 1408
TOK = 128
COLS = 512
NG = 8
NZ = 8
NX = 4
norm_eps = 1e-06
very_low = -1e30
MESH = pl.DeviceIdType.MESH
f32 = jnp.float32
bf16 = jnp.bfloat16


def row_of(col, eye):
    return jnp.sum(jnp.where(eye, col, 0.0), axis=0, keepdims=True)


def col_of(row, eye):
    return jnp.sum(jnp.where(eye, row, 0.0), axis=1, keepdims=True)


def split_hi_lo(x):
    hi = x.astype(bf16)
    return hi, (x - hi.astype(f32)).astype(bf16)


def dot(a, b, dims=((1,), (0,))):
    return lax.dot_general(a, b, (dims, ((), ())), preferred_element_type=f32)


def log_sigmoid(x):
    return jnp.minimum(x, 0.0) - jnp.log1p(jnp.exp(-jnp.abs(x)))


def copy_to(src, dst, ssem, rsem, dev):
    return pltpu.make_async_remote_copy(
        src_ref=src, dst_ref=dst, send_sem=ssem, recv_sem=rsem, device_id=dev, device_id_type=MESH
    )


def barrier_all(devs):
    bar = pltpu.get_barrier_semaphore()
    for dev in devs:
        pl.semaphore_signal(bar, inc=1, device_id=dev, device_id_type=MESH)
    return bar, len(devs)


def cell_kernel(
    q_ref,
    k_ref,
    v_ref,
    og_ref,
    ig_ref,
    fg_ref,
    hg_ref,
    wo_ref,
    st_ref,
    gain_ref,
    y_ref,
    r_ref,
    resid_ref,
    small1,
    small2,
    small_l,
    small_me,
    small_t,
    s_loc,
    r1,
    pre_l,
    t_loc,
    r2,
    o3,
    r3,
    part,
    rpart,
    sq_me,
    rsq,
    yloc,
    ss,
    rs,
):
    sp, tp = lax.axis_index("sp"), lax.axis_index("tp")
    z, g = sp // NG, lax.rem(sp, NG)
    gpeer = [lax.rem(g + r, NG) for r in range(NG)]
    gfrom = [lax.rem(g + NG - r, NG) for r in range(NG)]
    zpeer = [lax.rem(z + r, NZ) for r in range(NZ)]
    xpeer = [lax.rem(tp + r, NX) for r in range(NX)]
    xfrom = [lax.rem(tp + NX - r, NX) for r in range(NX)]
    gdev = [{"sp": z * NG + p, "tp": tp} for p in gpeer]
    zdev = [{"sp": p * NG + g, "tp": tp} for p in zpeer]
    xdev = [{"sp": sp, "tp": p} for p in xpeer]
    bar, count = barrier_all(gdev[1:] + zdev[1:] + xdev[1:])

    rows = lax.broadcasted_iota(jnp.int32, (TOK, TOK), 0)
    cols = lax.broadcasted_iota(jnp.int32, (TOK, TOK), 1)
    eye = rows == cols
    low = rows >= cols

    lf = log_sigmoid(fg_ref[...])
    ig = ig_ref[...]
    small_me[...] = jnp.zeros_like(small_me)
    cs_cols, pairs, wks = [], [], []
    for h in range(2):
        lf_col = lf[:, h : h + 1]
        lf_row = row_of(lf_col, eye)
        cs_col = jnp.sum(jnp.where(low, lf_row, 0.0), axis=1, keepdims=True)
        cs_row = jnp.sum(jnp.where(rows <= cols, lf_col, 0.0), axis=0, keepdims=True)
        ig_col = ig[:, h : h + 1]
        ig_row = row_of(ig_col, eye)
        rest_row = ig_row - cs_row
        rest_col = ig_col - cs_col
        top = jnp.max(rest_row, axis=1, keepdims=True)
        total = jnp.sum(lf_row, axis=1, keepdims=True)
        wk = jnp.exp(rest_col - top) * k_ref[:, h * DQK : (h + 1) * DQK].astype(f32)
        small_me[h : h + 1, :] = jnp.sum(wk, axis=0, keepdims=True)
        small_me[2 + h : 3 + h, :] = jnp.broadcast_to(total, (1, TOK))
        small_me[4 + h : 5 + h, :] = jnp.broadcast_to(total + top, (1, TOK))
        cs_cols.append(cs_col)
        pairs.append((rest_row, ig_row))
        wks.append(wk)
    pl.semaphore_wait(bar, count)
    pending = []
    for r in range(1, NG):
        c = copy_to(small_me, small1.at[g], ss.at[0, r], rs.at[0, r], gdev[r])
        c.start()
        pending.append(c)
    small1[g] = small_me[...]

    for h in range(2):
        hi, lo = split_hi_lo(wks[h])
        v_h = v_ref[:, h * DV : (h + 1) * DV]
        state = dot(hi, v_h, ((0,), (0,))) + dot(lo, v_h, ((0,), (0,)))
        s_loc[4 * h : 4 * h + 4] = state.astype(bf16).reshape(4, 32, DV)
    for r in range(1, NG):
        c = copy_to(s_loc.at[gpeer[r]], r1.at[g], ss.at[1, r], rs.at[1, r], gdev[r])
        c.start()
        pending.append(c)
    r1[g] = s_loc[g]

    scale = DQK**-0.5
    num0, den0, peak0 = [], [], []
    for h in range(2):
        rest_row, ig_row = pairs[h]
        q_h = q_ref[:, h * DQK : (h + 1) * DQK]
        k_h = k_ref[:, h * DQK : (h + 1) * DQK]
        log_pair = jnp.where(low, cs_cols[h] + rest_row, -jnp.inf)
        peak = jnp.max(log_pair, axis=1, keepdims=True)
        scores = dot(q_h, k_h, ((1,), (1,))) * scale * jnp.exp(log_pair - peak)
        hi, lo = split_hi_lo(scores)
        v_h = v_ref[:, h * DV : (h + 1) * DV]
        num0.append(dot(hi, v_h) + dot(lo, v_h))
        den0.append(jnp.sum(scores, axis=1, keepdims=True))
        peak0.append(peak)

    for r in range(1, NG):
        pltpu.make_async_remote_copy(
            small_me, small1.at[gfrom[r]], ss.at[0, r], rs.at[0, r], gdev[r], MESH
        ).wait_recv()
    n_l = jnp.zeros((2, TOK), f32)
    a_l = jnp.zeros((2, TOK), f32)
    m_l = jnp.full((2, TOK), very_low, f32)
    a_list, m_list, f_list, l_list = [], [], [], []
    for i in range(NG):
        small_l[i, 0:2, :] = n_l
        small_l[i, 2:4, :] = a_l
        small_l[i, 4:6, :] = m_l
        a_list.append(a_l)
        m_list.append(m_l)
        n_i, a_i, m_i = small1[i, 0:2, :], small1[i, 2:4, :], small1[i, 4:6, :]
        new = jnp.maximum(a_i + m_l, m_i)
        former, latter = jnp.exp(a_i + m_l - new), jnp.exp(m_i - new)
        f_list.append(former)
        l_list.append(latter)
        n_l = former * n_l + latter * n_i
        a_l = a_l + a_i
        m_l = new
    small_t[...] = jnp.zeros_like(small_t)
    small_t[0:2, :] = n_l
    small_t[2:4, :] = a_l
    small_t[4:6, :] = m_l
    for r in range(1, NZ):
        c = copy_to(small_t, small2.at[z], ss.at[2, r], rs.at[2, r], zdev[r])
        c.start()
        pending.append(c)
    small2[z] = small_t[...]

    def mine(pair):
        return jnp.where(g < 4, pair[0:1, :], pair[1:2, :])

    def spread(line):
        return jnp.concatenate([line, line], axis=1)

    for r in range(1, NG):
        copy_to(s_loc.at[0], r1.at[gfrom[r]], ss.at[1, r], rs.at[1, r], gdev[r]).wait_recv()
    run = jnp.zeros((32, DV), f32)
    for i in range(NG):
        pre_l[i] = run
        run = spread(mine(f_list[i])) * run + spread(mine(l_list[i])) * r1[i].astype(f32)
    t_loc[...] = run.astype(bf16)
    for r in range(1, NZ):
        c = copy_to(t_loc, r2.at[z], ss.at[3, r], rs.at[3, r], zdev[r])
        c.start()
        pending.append(c)
    r2[z] = t_loc[...]

    for r in range(1, NZ):
        copy_to(
            small_t, small2.at[lax.rem(z + NZ - r, NZ)], ss.at[2, r], rs.at[2, r], zdev[r]
        ).wait_recv()
    n_z = jnp.zeros((2, TOK), f32)
    m_z = jnp.full((2, TOK), very_low, f32)
    fz, lz = [], []
    for i in range(NZ):
        on = i < z
        n_i, a_i, m_i = small2[i, 0:2, :], small2[i, 2:4, :], small2[i, 4:6, :]
        new = jnp.maximum(a_i + m_z, m_i)
        former, latter = jnp.exp(a_i + m_z - new), jnp.exp(m_i - new)
        former = jnp.where(on, former, 1.0)
        latter = jnp.where(on, latter, 0.0)
        fz.append(mine(former))
        lz.append(mine(latter))
        n_z = former * n_z + latter * n_i
        m_z = jnp.where(on, new, m_z)
    ca, cb = [], []
    for j in range(NG):
        new = jnp.maximum(a_list[j] + m_z, m_list[j])
        ca.append(mine(jnp.exp(m_list[j] - new)))
        cb.append(mine(jnp.exp(a_list[j] + m_z - new)))
    n_g, a_g, m_g = small_l[g, 0:2, :], small_l[g, 2:4, :], small_l[g, 4:6, :]
    m_in = jnp.maximum(a_g + m_z, m_g)
    n_in = jnp.exp(m_g - m_in) * n_g + jnp.exp(a_g + m_z - m_in) * n_z

    scale0, carried, denom = [], [], []
    for h in range(2):
        q_h = q_ref[:, h * DQK : (h + 1) * DQK].astype(f32)
        log_carry = cs_cols[h] + m_in[h : h + 1, 0:1]
        peak = jnp.maximum(peak0[h], log_carry)
        s0, c0 = jnp.exp(peak0[h] - peak), jnp.exp(log_carry - peak) * scale
        normer = s0 * den0[h] + c0 * jnp.sum(q_h * n_in[h : h + 1, :], axis=1, keepdims=True)
        inv = 1.0 / jnp.maximum(jnp.abs(normer), jnp.exp(-peak))
        scale0.append(s0 * inv)
        carried.append(c0 * inv)

    for r in range(1, NZ):
        copy_to(
            t_loc, r2.at[lax.rem(z + NZ - r, NZ)], ss.at[3, r], rs.at[3, r], zdev[r]
        ).wait_recv()
    run = jnp.zeros((32, DV), f32)
    for i in range(NZ):
        run = spread(fz[i]) * run + spread(lz[i]) * r2[i].astype(f32)
    for j in range(NG):
        o3[j] = (spread(ca[j]) * pre_l[j] + spread(cb[j]) * run).astype(bf16)
    for r in range(1, NG):
        c = copy_to(o3.at[gpeer[r]], r3.at[g], ss.at[4, r], rs.at[4, r], gdev[r])
        c.start()
        pending.append(c)
    r3[g] = o3[g]
    gates = [
        hg_ref[:, h * DV : (h + 1) * DV]
        / (1.0 + jnp.exp(-og_ref[:, h * DV : (h + 1) * DV].astype(f32)))
        for h in range(2)
    ]
    for r in range(1, NG):
        copy_to(o3.at[0], r3.at[gfrom[r]], ss.at[4, r], rs.at[4, r], gdev[r]).wait_recv()
    gated, sq = [], jnp.zeros((TOK, 1), f32)
    for h in range(2):
        q_h = q_ref[:, h * DQK : (h + 1) * DQK]
        state = r3[4 * h : 4 * h + 4].reshape(DQK, DV)
        out = scale0[h] * num0[h] + carried[h] * dot(q_h, state)
        sq = sq + jnp.sum(out * out, axis=1, keepdims=True)
        gated.append((out * gates[h]).astype(bf16))
    sq_me[0] = jnp.broadcast_to(row_of(sq, eye), (8, TOK))
    for r in range(1, NX):
        c = copy_to(sq_me.at[0], rsq.at[0, tp], ss.at[5, r], rs.at[5, r], xdev[r])
        c.start()
        pending.append(c)
    rsq[0, tp] = sq_me[0]
    heads = jnp.concatenate(gated, axis=1)
    for r in (2, 1, 3, 0):
        at = pl.multiple_of(xpeer[r] * COLS, COLS)
        part[xpeer[r]] = dot(heads, wo_ref[:, pl.ds(at, COLS)]).astype(bf16)
        if r:
            c = copy_to(part.at[xpeer[r]], rpart.at[tp], ss.at[6, r], rs.at[6, r], xdev[r])
            c.start()
            pending.append(c)
    rpart[tp] = part[tp]
    for r in range(1, NX):
        copy_to(sq_me.at[0], rsq.at[0, xfrom[r]], ss.at[5, r], rs.at[5, r], xdev[r]).wait_recv()
    sq_all = jnp.sum(rsq[0, :, 0, :], axis=0, keepdims=True)
    row_scale = col_of(lax.rsqrt(sq_all / VALS + norm_eps), eye)
    for r in range(1, NX):
        copy_to(part.at[0], rpart.at[xfrom[r]], ss.at[6, r], rs.at[6, r], xdev[r]).wait_recv()
    mixer = rpart[0].astype(f32)
    for i in range(1, NX):
        mixer = mixer + rpart[i].astype(f32)
    resid = (st_ref[...].astype(f32) + mixer * row_scale).astype(bf16)
    resid_ref[...] = resid
    resid_f = resid.astype(f32)
    gain = gain_ref[:, pl.ds(pl.multiple_of(tp * COLS, COLS), COLS)]
    yloc[...] = (resid_f * gain).astype(bf16)
    sq_me[1] = jnp.broadcast_to(
        row_of(jnp.sum(resid_f * resid_f, axis=1, keepdims=True), eye), (8, TOK)
    )
    for r in (2, 1, 3):
        c = copy_to(yloc, y_ref.at[tp], ss.at[8, r], rs.at[8, r], xdev[r])
        c.start()
        pending.append(c)
    for r in range(1, NX):
        c = copy_to(sq_me.at[1], rsq.at[1, tp], ss.at[7, r], rs.at[7, r], xdev[r])
        c.start()
        pending.append(c)
    rsq[1, tp] = sq_me[1]
    y_ref[tp] = yloc[...]
    for r in range(1, NX):
        copy_to(sq_me.at[1], rsq.at[1, xfrom[r]], ss.at[7, r], rs.at[7, r], xdev[r]).wait_recv()
    sq_all = jnp.sum(rsq[1, :, 0, :], axis=0, keepdims=True)
    r_ref[...] = jnp.broadcast_to(
        col_of(lax.rsqrt(sq_all / D + norm_eps), eye), (TOK, TOK)
    )
    for r in range(1, NX):
        copy_to(yloc, y_ref.at[xfrom[r]], ss.at[8, r], rs.at[8, r], xdev[r]).wait_recv()
    for c in pending:
        c.wait_send()


def ffn_kernel(y_ref, r_ref, resid_ref, w_hbm, o_ref, w, acc, part, rpart, lsem, ss, rs):
    sp, tp = lax.axis_index("sp"), lax.axis_index("tp")
    xpeer = [lax.rem(tp + r, NX) for r in range(NX)]
    xfrom = [lax.rem(tp + NX - r, NX) for r in range(NX)]
    xdev = [{"sp": sp, "tp": p} for p in xpeer]
    loads = []
    for i in range(NX):
        loads.append(
            pltpu.make_async_copy(
                w_hbm.at[pl.ds(i * COLS, COLS), pl.ds(0, 2 * FFT)],
                w.at[pl.ds(i * COLS, COLS), pl.ds(0, 2 * FFT)],
                lsem.at[i],
            )
        )
    for i in range(NX):
        loads.append(
            pltpu.make_async_copy(
                w_hbm.at[pl.ds(i * COLS, COLS), pl.ds(2 * FFT, FFT)],
                w.at[pl.ds(i * COLS, COLS), pl.ds(2 * FFT, FFT)],
                lsem.at[NX + i],
            )
        )
    for c in loads:
        c.start()
    bar, count = barrier_all(xdev[1:])
    pl.semaphore_wait(bar, count)
    for i in range(NX):
        loads[i].wait()
        term = dot(y_ref[i], w[i * COLS : (i + 1) * COLS, 0 : 2 * FFT])
        if i == 0:
            acc[...] = term
        else:
            acc[...] += term
    scale = r_ref[:, 0:1]
    gate = acc[:, 0:FFT] * scale
    hidden = (gate / (1.0 + jnp.exp(-gate)) * (acc[:, FFT:] * scale)).astype(bf16)
    for i in range(NX):
        loads[NX + i].wait()
    pending = []
    for r in (2, 1, 3, 0):
        at = pl.multiple_of(xpeer[r] * COLS, COLS)
        part[xpeer[r]] = dot(
            hidden, w[pl.ds(at, COLS), 2 * FFT : 3 * FFT], ((1,), (1,))
        ).astype(bf16)
        if r:
            c = copy_to(part.at[xpeer[r]], rpart.at[tp], ss.at[r], rs.at[r], xdev[r])
            c.start()
            pending.append(c)
    total = resid_ref[...].astype(f32) + part[tp].astype(f32)
    for r in (1, 3, 2):
        copy_to(part.at[0], rpart.at[xfrom[r]], ss.at[r], rs.at[r], xdev[r]).wait_recv()
        total = total + rpart[xfrom[r]].astype(f32)
    o_ref[...] = total.astype(bf16)
    for c in pending:
        c.wait_send()


def local(
    stream,
    queries,
    keys,
    values,
    out_gate,
    input_gate,
    forget_gate,
    head_gain,
    w_out,
    ffn_gain,
    w_gate,
    w_up,
    w_down,
):
    vmem = pl.BlockSpec(memory_space=pltpu.VMEM)
    both = jnp.concatenate([w_gate, w_up, w_down.T], axis=1)
    weights = lax.all_gather(both, "sp", axis=0, tiled=True)
    y, r, resid = pl.pallas_call(
        cell_kernel,
        out_shape=(
            jax.ShapeDtypeStruct((NX, TOK, COLS), bf16),
            jax.ShapeDtypeStruct((TOK, TOK), f32),
            jax.ShapeDtypeStruct((TOK, COLS), bf16),
        ),
        in_specs=[vmem] * 10,
        out_specs=(vmem, vmem, vmem),
        scratch_shapes=[
            pltpu.VMEM((NG, 8, TOK), f32),
            pltpu.VMEM((NZ, 8, TOK), f32),
            pltpu.VMEM((NG, 8, TOK), f32),
            pltpu.VMEM((8, TOK), f32),
            pltpu.VMEM((8, TOK), f32),
            pltpu.VMEM((NG, 32, DV), bf16),
            pltpu.VMEM((NG, 32, DV), bf16),
            pltpu.VMEM((NG, 32, DV), f32),
            pltpu.VMEM((32, DV), bf16),
            pltpu.VMEM((NZ, 32, DV), bf16),
            pltpu.VMEM((NG, 32, DV), bf16),
            pltpu.VMEM((NG, 32, DV), bf16),
            pltpu.VMEM((NX, TOK, COLS), bf16),
            pltpu.VMEM((NX, TOK, COLS), bf16),
            pltpu.VMEM((2, 8, TOK), f32),
            pltpu.VMEM((2, NX, 8, TOK), f32),
            pltpu.VMEM((TOK, COLS), bf16),
            pltpu.SemaphoreType.DMA((9, 8)),
            pltpu.SemaphoreType.DMA((9, 8)),
        ],
        compiler_params=pltpu.CompilerParams(collective_id=0, has_side_effects=True),
        cost_estimate=pl.CostEstimate(flops=50_000_000_000, bytes_accessed=4_000_000, transcendentals=0),
    )(
        queries,
        keys,
        values,
        out_gate,
        input_gate,
        forget_gate,
        head_gain.reshape(1, COLS),
        w_out,
        stream,
        ffn_gain.reshape(1, D),
    )
    return pl.pallas_call(
        ffn_kernel,
        out_shape=jax.ShapeDtypeStruct((TOK, COLS), bf16),
        in_specs=[vmem, vmem, vmem, pl.BlockSpec(memory_space=pl.ANY)],
        out_specs=vmem,
        scratch_shapes=[
            pltpu.VMEM((D, 3 * FFT), bf16),
            pltpu.VMEM((TOK, 2 * FFT), f32),
            pltpu.VMEM((NX, TOK, COLS), bf16),
            pltpu.VMEM((NX, TOK, COLS), bf16),
            pltpu.SemaphoreType.DMA((8,)),
            pltpu.SemaphoreType.DMA((NX,)),
            pltpu.SemaphoreType.DMA((NX,)),
        ],
        compiler_params=pltpu.CompilerParams(collective_id=1, has_side_effects=True, vmem_limit_bytes=56 * 2**20),
    )(y, r, resid, weights)


def solution(mesh):
    in_specs = (
        P("sp", "tp"),
        P("sp", "tp"),
        P("sp", "tp"),
        P("sp", "tp"),
        P("sp", "tp"),
        P("sp", "tp"),
        P("sp", "tp"),
        P("tp"),
        P("tp", None),
        P(),
        P("sp", "tp"),
        P("sp", "tp"),
        P("tp", "sp"),
    )
    return jax.shard_map(
        local, mesh=mesh, in_specs=in_specs, out_specs=P("sp", "tp"), check_vma=False
    )
```

time: 232 us -> 142 us (0.61)
  Pallas kernels: 0 us -> 63.4 us
  waiting for transfers between devices: 113 us -> 58.9 us
  blocking collectives: 36.5 us -> 0 us
  other arithmetic: 22.5 us -> 1.7 us
  matrix products: 16.5 us -> 0 us
  local copies, waits for them, and re-layouts: 20.5 us -> 4.39 us
  starting transfers between devices: 6.98 us -> 0.01 us
    pallas_call x0 -> x2, Pallas kernels: none -> 63.4 us  [the longest x1 45.3 us: local(): pl.pallas_call(cell_kernel, out_shape=(jax.ShapeDtypeStruct((NX, TOK, COL...]
    all_gather x3 -> x1, waiting for transfers between devices: 106 us -> 58.9 us  [local(): weights = lax.all_gather(both, 'sp', axis=0, tiled=True)]
    all_to_all x3 -> x0, blocking collectives: 31.5 us -> none  [the longest x2 22.1 us: summed_on_arrival(): lax.all_to_all(parts, axis, split_axis=0, concat_axis=0, tiled=True)]
    dot_general x9 -> x0, matrix products: 16.5 us -> none  [the longest x1 7.41 us: local(): term = jnp.dot(hidden, down_full, preferred_element_type=jnp.float32)]
    slice x10 -> x0, local copies, waits for them, and re-layouts: 8.34 us -> none  [the longest x6 6.41 us: entering(): subtotal = combine(subtotal, jax.tree.map(lambda part: part[k], pieces))]
    exp x21 -> x0, other arithmetic: 7.15 us -> none  [the longest x10 4.19 us: combine(): former = jnp.exp(later[3] + earlier[2] - ceiling)]
    all_to_all x2 -> x0, waiting for transfers between devices: 7.08 us -> none  [copy_for_each(): lax.all_to_all(jnp.broadcast_to(x[None], (peers, *x.shape)), axis, 0, 0,...]
    all_to_all x2 -> x0, starting transfers between devices: 6.89 us -> none  [copy_for_each(): lax.all_to_all(jnp.broadcast_to(x[None], (peers, *x.shape)), axis, 0, 0,...]
  transfers between devices with their start and end apart: 5 -> 1, of which waited for: 5 -> 1; matrix products, arithmetic and copies ran while one was open for 14% -> 2% of each run, Pallas kernels for 0% -> 32%
where the time goes in v1:
time: 142 us
  Pallas kernels  63.4 us (45%)
  waiting for transfers between devices  58.9 us (41%)
  between operations  13.4 us (9%)
  local copies, waits for them, and re-layouts  4.39 us (3%)
  other arithmetic  1.7 us (1%)
    all_gather x1, waiting for transfers between devices, local(): weights = lax.all_gather(both, 'sp', axis=0, tiled=True)  58.9 us
    pallas_call x1, Pallas kernels, local(): pl.pallas_call(cell_kernel, out_shape=(jax.ShapeDtypeStruct((NX, TOK, COL...  45.3 us
    pallas_call x1, Pallas kernels, local(): pl.pallas_call(ffn_kernel, out_shape=jax.ShapeDtypeStruct((TOK, COLS), bf...  18.1 us
    unnamed x3, local copies, waits for them, and re-layouts  4.39 us
  transfers between devices with their start and end apart: 1, of which 1 were waited for; matrix products, arithmetic and copies ran while one was open for 2% of the time, Pallas kernels for 32%

profile of v1, /device:TPU:1, one launch (start us, length us, event | category | flops | bytes accessed | tf_op | source)
XLA Modules:
  0.0 141.8 jit_solution(12064772343464625056)
XLA Ops:
  6.5 0.0 all-gather.2.cloned.1.call-start
  6.5 1.7 %pad_maximum_fusion = bf16[32,4224]{1,0:T(8,128)(2,1)} fusion(bf16[32,1408]{1,0:T(8,128)(2,1)} %bitcast.3, bf16[32,1408]{1,0:T(8,128)(2,1)} %param.24, bf16[32,1408]{1,0:T(8,128)(2,1)} %param.23), kind=kLoop, calls=%fused_computation | loop fusion | flops 811008 | bytes 540672 | tf_op jit(solution)/shard_map/concatenate | solution.py:412
  8.2 0.0 all-gather.2.cloned.1.call-update
  8.3 1.4 copy.14.ig_ref
  9.7 1.4 copy.15.fg_ref
  11.1 45.3 %shard_map.127 = (bf16[4,128,512]{2,1,0:T(8,128)(2,1)}, f32[128,128]{1,0:T(8,128)}, bf16[128,512]{1,0:T(8,128)(2,1)}) custom-call(bf16[128,256]{1,0:T(8,128)(2,1)} %q_ref.1, bf16[128,256]{1,0:T(8,128)(2,1)} %k_ref.1, bf16[128,512]{1,0:T(8,128)(2,1)} %v_ref.1, bf16[128,512]{1,0:T(8,128)(2,1)} %og_ref.1, f32[128,2]{1,0:T(8,128)} %copy.14.ig_ref, ...), custom_call_target="tpu_custom_call" | custom-call | flops 49999998976 | bytes 4000000 | tf_op jit(solution)/shard_map/pallas_call | solution.py:414
  56.4 58.9 %all-gather.2.cloned.1.call-done.w_hbm = bf16[2048,4224]{1,0:T(8,128)(2,1)} async-done(((bf16[32,4224]{1,0:T(8,128)(2,1)}), bf16[2048,4224]{1,0:T(8,128)(2,1)}) %all-gather.2.cloned.1.call-update) | async-done | bytes 17301520 | tf_op jit(solution)/shard_map/all_gather | solution.py:413
  115.3 18.1 %shard_map.128 = bf16[128,512]{1,0:T(8,128)(2,1)} custom-call(bf16[4,128,512]{2,1,0:T(8,128)(2,1)} %get-tuple-element.8.y_ref, f32[128,128]{1,0:T(8,128)} %get-tuple-element.9.r_ref, bf16[128,512]{1,0:T(8,128)(2,1)} %get-tuple-element.10.resid_ref, bf16[2048,4224]{1,0:T(8,128)(2,1)} %all-gather.2.cloned.1.call-done.w_hbm), custom_call_target="tpu_custom_call" | custom-call | tf_op jit(solution)/shard_map/pallas_call | solution.py:458
  133.4 1.6 %copy.17 = bf16[128,512]{1,0:T(8,128)(2,1)} copy(bf16[128,512]{1,0:T(8,128)(2,1)} %shard_map.128) | data formatting | bytes 262144
Async XLA Ops:
  6.5 108.7 %all-gather.2.cloned.1.call-start = ((), (), s32[]{:S(2)}) async-start(), calls=%async_computation | async-start | bytes 17571840 | tf_op jit(solution)/shard_map/all_gather | solution.py:413
Sparse Core Ops, SparseCore 0:
  10.1 105.1 all-gather.1

commit v2 on v1

--- a/solution.py
+++ b/solution.py
@@ -58,7 +58,169 @@
     return bar, len(devs)
 
 
-def cell_kernel(
+class Weights:
+    def __init__(self, w, wss, wrs, z, g, tp):
+        self.w, self.wss, self.wrs = w, wss, wrs
+        self.z, self.y, self.c, self.tp = z, g // 2, lax.rem(g, 2), tp
+        self.ids, self.sent = {}, []
+        self.zi = [lax.rem(z + k, NZ) for k in (0, 7, 1, 6, 2, 5, 3, 4)]
+        z_at = lambda k: {"sp": lax.rem(z + k, NZ) * NG + g, "tp": tp}
+        y_at = lambda k: {"sp": z * NG + lax.rem(self.y + k, 4) * 2 + self.c, "tp": tp}
+        self.dev = {
+            "z+": z_at(1),
+            "z-": z_at(7),
+            "y+": y_at(1),
+            "y-": y_at(3),
+            "s": {"sp": z * NG + self.y * 2 + (1 - self.c), "tp": tp},
+        }
+
+    def zk(self, k):
+        return lax.rem(self.z + NZ + k, NZ)
+
+    def yk(self, k):
+        return lax.rem(self.y + 4 + k, 4)
+
+    def both(self, zi, yi):
+        return (pl.ds(0, 2), zi, yi, self.c)
+
+    def desc(self, name, way, at):
+        n = self.ids.setdefault((name, way), len(self.ids))
+        return copy_to(self.w.at[at], self.w.at[at], self.wss.at[n], self.wrs.at[n], self.dev[way])
+
+    def send(self, name, way, at):
+        c = self.desc(name, way, at)
+        c.start()
+        self.sent.append(c)
+
+    def got(self, name, way, at):
+        self.desc(name, way, at).wait_recv()
+
+    def first(self):
+        own = self.both(self.z, self.y)
+        self.send("bz1", "z+", own)
+        self.send("bz1", "z-", own)
+        down = (2, self.z, self.y, self.c)
+        self.send("ay", "y+", down)
+        self.send("ay", "y-", down)
+        self.by(0)
+
+    def bz(self, k):
+        back, ahead = self.zk(-k), self.zk(k)
+        if k == 4:
+            self.got("bz4", "z+", (0, back, self.y, self.c))
+            self.got("bz4", "z-", (1, ahead, self.y, self.c))
+            return
+        self.got(f"bz{k}", "z+", self.both(back, self.y))
+        self.got(f"bz{k}", "z-", self.both(ahead, self.y))
+        if k == 3:
+            self.send("bz4", "z+", (0, back, self.y, self.c))
+            self.send("bz4", "z-", (1, ahead, self.y, self.c))
+        else:
+            self.send(f"bz{k + 1}", "z+", self.both(back, self.y))
+            self.send(f"bz{k + 1}", "z-", self.both(ahead, self.y))
+
+    def by(self, j):
+        self.send(f"by{j}", "y+", self.both(self.zi[j], self.y))
+        self.send(f"by{j}", "y-", self.both(self.zi[j], self.y))
+
+    def byf(self, j):
+        self.got(f"by{j}", "y+", self.both(self.zi[j], self.yk(-1)))
+        self.send(f"byf{j}", "y+", (0, self.zi[j], self.yk(-1), self.c))
+        self.got(f"by{j}", "y-", self.both(self.zi[j], self.yk(1)))
+        self.send(f"byf{j}", "y-", (1, self.zi[j], self.yk(1), self.c))
+
+    def sb(self, j):
+        self.got(f"byf{j}", "y+", (0, self.zi[j], self.yk(-2), self.c))
+        self.got(f"byf{j}", "y-", (1, self.zi[j], self.yk(2), self.c))
+        self.send(f"sb{j}", "s", (pl.ds(0, 2), self.zi[j], pl.ds(0, 4), self.c))
+
+    def ayf(self):
+        self.got("ay", "y+", (2, self.z, self.yk(-1), self.c))
+        self.send("ayf", "y+", (2, self.z, self.yk(-1), self.c, pl.ds(0, 16)))
+        self.got("ay", "y-", (2, self.z, self.yk(1), self.c))
+        self.send("ayf", "y-", (2, self.z, self.yk(1), self.c, pl.ds(16, 16)))
+
+    def pair(self, zi, p):
+        return (2, zi, pl.ds(2 * p, 2), self.c)
+
+    def sa(self, k):
+        self.send(f"sa{k}", "s", (2, self.zk(k), pl.ds(0, 4), self.c))
+
+    def az(self, k):
+        if k == 0:
+            self.got("ayf", "y+", (2, self.z, self.yk(-2), self.c, pl.ds(0, 16)))
+            self.got("ayf", "y-", (2, self.z, self.yk(2), self.c, pl.ds(16, 16)))
+        back, ahead = self.zk(-k), self.zk(k)
+        if k == 4:
+            self.got("az4", "z+", self.pair(back, 0))
+            self.got("az4", "z-", self.pair(ahead, 1))
+            self.sa(4)
+            return
+        for p in range(2):
+            if k:
+                self.got(f"az{k}{p}", "z+", self.pair(back, p))
+            if k < 3:
+                self.send(f"az{k + 1}{p}", "z+", self.pair(back, p))
+            elif p == 0:
+                self.send("az4", "z+", self.pair(back, 0))
+            if k:
+                self.got(f"az{k}{p}", "z-", self.pair(ahead, p))
+            if k < 3:
+                self.send(f"az{k + 1}{p}", "z-", self.pair(ahead, p))
+            elif p == 1:
+                self.send("az4", "z-", self.pair(ahead, 1))
+        self.sa(-k)
+        if k:
+            self.sa(k)
+
+    def after_slices(self):
+        self.bz(1)
+        self.ayf()
+        self.byf(0)
+        self.by(1)
+        self.by(2)
+
+    def after_totals(self):
+        self.bz(2)
+        self.az(0)
+
+    def after_prefixes(self):
+        self.bz(3)
+        for j in (3, 4, 5, 6):
+            self.by(j)
+        self.byf(1)
+        self.byf(2)
+
+    def after_partials(self):
+        self.bz(4)
+        self.by(7)
+        self.az(1)
+        self.sb(0)
+
+    def after_features(self):
+        self.az(2)
+        for j in (1, 2):
+            self.sb(j)
+        for j in (3, 4):
+            self.byf(j)
+
+    def before_column(self, j):
+        if j == 0:
+            self.az(3)
+            for k in (5, 6, 7):
+                self.byf(k)
+        if j >= 3:
+            self.sb(j)
+        if j == 5:
+            self.az(4)
+        self.got(f"sb{j}", "s", (pl.ds(0, 2), self.zi[j], pl.ds(0, 4), 1 - self.c))
+
+    def before_down(self):
+        for k in (0, -1, 1, -2, 2, -3, 3, 4):
+            self.got(f"sa{k}", "s", (2, self.zk(k), pl.ds(0, 4), 1 - self.c))
+
+
+def layer_kernel(
     q_ref,
     k_ref,
     v_ref,
@@ -66,12 +228,17 @@
     ig_ref,
     fg_ref,
     hg_ref,
-    wo_ref,
+    wo_hbm,
     st_ref,
     gain_ref,
+    wg_hbm,
+    wu_hbm,
+    wd_hbm,
+    o_ref,
+    w,
+    wo,
+    acc,
     y_ref,
-    r_ref,
-    resid_ref,
     small1,
     small2,
     small_l,
@@ -89,8 +256,13 @@
     sq_me,
     rsq,
     yloc,
+    part2,
+    rpart2,
+    lsem,
     ss,
     rs,
+    wss,
+    wrs,
 ):
     sp, tp = lax.axis_index("sp"), lax.axis_index("tp")
     z, g = sp // NG, lax.rem(sp, NG)
@@ -103,6 +275,14 @@
     zdev = [{"sp": p * NG + g, "tp": tp} for p in zpeer]
     xdev = [{"sp": sp, "tp": p} for p in xpeer]
     bar, count = barrier_all(gdev[1:] + zdev[1:] + xdev[1:])
+    net = Weights(w, wss, wrs, z, g, tp)
+    loads = [
+        pltpu.make_async_copy(ref, w.at[kind, z, net.y, net.c], lsem.at[kind])
+        for kind, ref in enumerate((wg_hbm, wu_hbm, wd_hbm))
+    ]
+    loads.append(pltpu.make_async_copy(wo_hbm, wo, lsem.at[3]))
+    for c in loads:
+        c.start()
 
     rows = lax.broadcasted_iota(jnp.int32, (TOK, TOK), 0)
     cols = lax.broadcasted_iota(jnp.int32, (TOK, TOK), 1)
@@ -114,14 +294,13 @@
     small_me[...] = jnp.zeros_like(small_me)
     cs_cols, pairs, wks = [], [], []
     for h in range(2):
-        lf_col = lf[:, h : h + 1]
-        lf_row = row_of(lf_col, eye)
+        lf_row = lf[h : h + 1, :]
+        lf_col = col_of(lf_row, eye)
         cs_col = jnp.sum(jnp.where(low, lf_row, 0.0), axis=1, keepdims=True)
         cs_row = jnp.sum(jnp.where(rows <= cols, lf_col, 0.0), axis=0, keepdims=True)
-        ig_col = ig[:, h : h + 1]
-        ig_row = row_of(ig_col, eye)
+        ig_row = ig[h : h + 1, :]
         rest_row = ig_row - cs_row
-        rest_col = ig_col - cs_col
+        rest_col = col_of(rest_row, eye)
         top = jnp.max(rest_row, axis=1, keepdims=True)
         total = jnp.sum(lf_row, axis=1, keepdims=True)
         wk = jnp.exp(rest_col - top) * k_ref[:, h * DQK : (h + 1) * DQK].astype(f32)
@@ -138,6 +317,9 @@
         c.start()
         pending.append(c)
     small1[g] = small_me[...]
+    for c in loads[:3]:
+        c.wait()
+    net.first()
 
     for h in range(2):
         hi, lo = split_hi_lo(wks[h])
@@ -149,6 +331,7 @@
         c.start()
         pending.append(c)
     r1[g] = s_loc[g]
+    net.after_slices()
 
     scale = DQK**-0.5
     num0, den0, peak0 = [], [], []
@@ -215,6 +398,7 @@
         c.start()
         pending.append(c)
     r2[z] = t_loc[...]
+    net.after_totals()
 
     for r in range(1, NZ):
         copy_to(
@@ -268,6 +452,7 @@
         c.start()
         pending.append(c)
     r3[g] = o3[g]
+    net.after_prefixes()
     gates = [
         hg_ref[:, h * DV : (h + 1) * DV]
         / (1.0 + jnp.exp(-og_ref[:, h * DV : (h + 1) * DV].astype(f32)))
@@ -289,14 +474,16 @@
         pending.append(c)
     rsq[0, tp] = sq_me[0]
     heads = jnp.concatenate(gated, axis=1)
+    loads[3].wait()
     for r in (2, 1, 3, 0):
         at = pl.multiple_of(xpeer[r] * COLS, COLS)
-        part[xpeer[r]] = dot(heads, wo_ref[:, pl.ds(at, COLS)]).astype(bf16)
+        part[xpeer[r]] = dot(heads, wo[:, pl.ds(at, COLS)]).astype(bf16)
         if r:
             c = copy_to(part.at[xpeer[r]], rpart.at[tp], ss.at[6, r], rs.at[6, r], xdev[r])
             c.start()
             pending.append(c)
     rpart[tp] = part[tp]
+    net.after_partials()
     for r in range(1, NX):
         copy_to(sq_me.at[0], rsq.at[0, xfrom[r]], ss.at[5, r], rs.at[5, r], xdev[r]).wait_recv()
     sq_all = jnp.sum(rsq[0, :, 0, :], axis=0, keepdims=True)
@@ -307,7 +494,6 @@
     for i in range(1, NX):
         mixer = mixer + rpart[i].astype(f32)
     resid = (st_ref[...].astype(f32) + mixer * row_scale).astype(bf16)
-    resid_ref[...] = resid
     resid_f = resid.astype(f32)
     gain = gain_ref[:, pl.ds(pl.multiple_of(tp * COLS, COLS), COLS)]
     yloc[...] = (resid_f * gain).astype(bf16)
@@ -324,72 +510,41 @@
         pending.append(c)
     rsq[1, tp] = sq_me[1]
     y_ref[tp] = yloc[...]
+    net.after_features()
     for r in range(1, NX):
         copy_to(sq_me.at[1], rsq.at[1, xfrom[r]], ss.at[7, r], rs.at[7, r], xdev[r]).wait_recv()
     sq_all = jnp.sum(rsq[1, :, 0, :], axis=0, keepdims=True)
-    r_ref[...] = jnp.broadcast_to(
-        col_of(lax.rsqrt(sq_all / D + norm_eps), eye), (TOK, TOK)
-    )
+    scale_in = col_of(lax.rsqrt(sq_all / D + norm_eps), eye)
     for r in range(1, NX):
         copy_to(yloc, y_ref.at[xfrom[r]], ss.at[8, r], rs.at[8, r], xdev[r]).wait_recv()
-    for c in pending:
-        c.wait_send()
-
-
-def ffn_kernel(y_ref, r_ref, resid_ref, w_hbm, o_ref, w, acc, part, rpart, lsem, ss, rs):
-    sp, tp = lax.axis_index("sp"), lax.axis_index("tp")
-    xpeer = [lax.rem(tp + r, NX) for r in range(NX)]
-    xfrom = [lax.rem(tp + NX - r, NX) for r in range(NX)]
-    xdev = [{"sp": sp, "tp": p} for p in xpeer]
-    loads = []
-    for i in range(NX):
-        loads.append(
-            pltpu.make_async_copy(
-                w_hbm.at[pl.ds(i * COLS, COLS), pl.ds(0, 2 * FFT)],
-                w.at[pl.ds(i * COLS, COLS), pl.ds(0, 2 * FFT)],
-                lsem.at[i],
-            )
-        )
-    for i in range(NX):
-        loads.append(
-            pltpu.make_async_copy(
-                w_hbm.at[pl.ds(i * COLS, COLS), pl.ds(2 * FFT, FFT)],
-                w.at[pl.ds(i * COLS, COLS), pl.ds(2 * FFT, FFT)],
-                lsem.at[NX + i],
-            )
-        )
-    for c in loads:
-        c.start()
-    bar, count = barrier_all(xdev[1:])
-    pl.semaphore_wait(bar, count)
-    for i in range(NX):
-        loads[i].wait()
-        term = dot(y_ref[i], w[i * COLS : (i + 1) * COLS, 0 : 2 * FFT])
-        if i == 0:
-            acc[...] = term
-        else:
-            acc[...] += term
-    scale = r_ref[:, 0:1]
-    gate = acc[:, 0:FFT] * scale
-    hidden = (gate / (1.0 + jnp.exp(-gate)) * (acc[:, FFT:] * scale)).astype(bf16)
-    for i in range(NX):
-        loads[NX + i].wait()
-    pending = []
+    for j in range(NZ):
+        net.before_column(j)
+        zi = net.zi[j]
+        y_col = y_ref[zi // 2, :, pl.ds(pl.multiple_of(lax.rem(zi, 2) * 256, 256), 256)]
+        for kind in range(2):
+            term = dot(y_col, w[kind, zi].reshape(256, FFT))
+            if j == 0:
+                acc[kind] = term
+            else:
+                acc[kind] += term
+    gate = acc[0] * scale_in
+    hidden = (gate / (1.0 + jnp.exp(-gate)) * (acc[1] * scale_in)).astype(bf16)
+    net.before_down()
     for r in (2, 1, 3, 0):
-        at = pl.multiple_of(xpeer[r] * COLS, COLS)
-        part[xpeer[r]] = dot(
-            hidden, w[pl.ds(at, COLS), 2 * FFT : 3 * FFT], ((1,), (1,))
+        at = xpeer[r]
+        part2[at] = dot(
+            hidden, w[2, pl.ds(2 * at, 2)].reshape(COLS, FFT), ((1,), (1,))
         ).astype(bf16)
         if r:
-            c = copy_to(part.at[xpeer[r]], rpart.at[tp], ss.at[r], rs.at[r], xdev[r])
+            c = copy_to(part2.at[at], rpart2.at[tp], ss.at[9, r], rs.at[9, r], xdev[r])
             c.start()
             pending.append(c)
-    total = resid_ref[...].astype(f32) + part[tp].astype(f32)
+    total = resid_f + part2[tp].astype(f32)
     for r in (1, 3, 2):
-        copy_to(part.at[0], rpart.at[xfrom[r]], ss.at[r], rs.at[r], xdev[r]).wait_recv()
-        total = total + rpart[xfrom[r]].astype(f32)
+        copy_to(part2.at[0], rpart2.at[xfrom[r]], ss.at[9, r], rs.at[9, r], xdev[r]).wait_recv()
+        total = total + rpart2[xfrom[r]].astype(f32)
     o_ref[...] = total.astype(bf16)
-    for c in pending:
+    for c in pending + net.sent:
         c.wait_send()
 
 
@@ -409,18 +564,17 @@
     w_down,
 ):
     vmem = pl.BlockSpec(memory_space=pltpu.VMEM)
-    both = jnp.concatenate([w_gate, w_up, w_down.T], axis=1)
-    weights = lax.all_gather(both, "sp", axis=0, tiled=True)
-    y, r, resid = pl.pallas_call(
-        cell_kernel,
-        out_shape=(
-            jax.ShapeDtypeStruct((NX, TOK, COLS), bf16),
-            jax.ShapeDtypeStruct((TOK, TOK), f32),
-            jax.ShapeDtypeStruct((TOK, COLS), bf16),
-        ),
-        in_specs=[vmem] * 10,
-        out_specs=(vmem, vmem, vmem),
+    hbm = pl.BlockSpec(memory_space=pl.ANY)
+    return pl.pallas_call(
+        layer_kernel,
+        out_shape=jax.ShapeDtypeStruct((TOK, COLS), bf16),
+        in_specs=[vmem] * 7 + [hbm] + [vmem] * 2 + [hbm] * 3,
+        out_specs=vmem,
         scratch_shapes=[
+            pltpu.VMEM((3, NZ, 4, 2, 32, FFT), bf16),
+            pltpu.VMEM((COLS, D), bf16),
+            pltpu.VMEM((2, TOK, FFT), f32),
+            pltpu.VMEM((NX, TOK, COLS), bf16),
             pltpu.VMEM((NG, 8, TOK), f32),
             pltpu.VMEM((NZ, 8, TOK), f32),
             pltpu.VMEM((NG, 8, TOK), f32),
@@ -438,39 +592,32 @@
             pltpu.VMEM((2, 8, TOK), f32),
             pltpu.VMEM((2, NX, 8, TOK), f32),
             pltpu.VMEM((TOK, COLS), bf16),
-            pltpu.SemaphoreType.DMA((9, 8)),
-            pltpu.SemaphoreType.DMA((9, 8)),
+            pltpu.VMEM((NX, TOK, COLS), bf16),
+            pltpu.VMEM((NX, TOK, COLS), bf16),
+            pltpu.SemaphoreType.DMA((4,)),
+            pltpu.SemaphoreType.DMA((10, 8)),
+            pltpu.SemaphoreType.DMA((10, 8)),
+            pltpu.SemaphoreType.DMA((96,)),
+            pltpu.SemaphoreType.DMA((96,)),
         ],
-        compiler_params=pltpu.CompilerParams(collective_id=0, has_side_effects=True),
-        cost_estimate=pl.CostEstimate(flops=50_000_000_000, bytes_accessed=4_000_000, transcendentals=0),
+        compiler_params=pltpu.CompilerParams(
+            collective_id=0, has_side_effects=True, vmem_limit_bytes=60 * 2**20
+        ),
     )(
         queries,
         keys,
         values,
         out_gate,
-        input_gate,
-        forget_gate,
+        input_gate.T,
+        forget_gate.T,
         head_gain.reshape(1, COLS),
         w_out,
         stream,
         ffn_gain.reshape(1, D),
+        w_gate,
+        w_up,
+        w_down.T,
     )
-    return pl.pallas_call(
-        ffn_kernel,
-        out_shape=jax.ShapeDtypeStruct((TOK, COLS), bf16),
-        in_specs=[vmem, vmem, vmem, pl.BlockSpec(memory_space=pl.ANY)],
-        out_specs=vmem,
-        scratch_shapes=[
-            pltpu.VMEM((D, 3 * FFT), bf16),
-            pltpu.VMEM((TOK, 2 * FFT), f32),
-            pltpu.VMEM((NX, TOK, COLS), bf16),
-            pltpu.VMEM((NX, TOK, COLS), bf16),
-            pltpu.SemaphoreType.DMA((8,)),
-            pltpu.SemaphoreType.DMA((NX,)),
-            pltpu.SemaphoreType.DMA((NX,)),
-        ],
-        compiler_params=pltpu.CompilerParams(collective_id=1, has_side_effects=True, vmem_limit_bytes=56 * 2**20),
-    )(y, r, resid, weights)
 
 
 def solution(mesh):

time: 142 us -> 87.8 us (0.62)
  waiting for transfers between devices: 58.9 us -> 0 us
  Pallas kernels: 63.4 us -> 86.1 us
  between operations: 13.4 us -> 0.01 us
  local copies, waits for them, and re-layouts: 4.39 us -> 1.57 us
  other arithmetic: 1.7 us -> 0 us
    all_gather x1 -> x0, waiting for transfers between devices: 58.9 us -> none  [local(): weights = lax.all_gather(both, 'sp', axis=0, tiled=True)]
    pallas_call x2 -> x1, Pallas kernels: 63.4 us -> 86.1 us  [local(): pl.pallas_call(layer_kernel, out_shape=jax.ShapeDtypeStruct((TOK, COLS),...]
    unnamed x3 -> x1, local copies, waits for them, and re-layouts: 4.39 us -> 1.57 us
    concatenate x1 -> x0, other arithmetic: 1.7 us -> none  [local(): both = jnp.concatenate([w_gate, w_up, w_down.T], axis=1)]
  transfers between devices with their start and end apart: 1 -> 0, of which waited for: 1 -> 0; matrix products, arithmetic and copies ran while one was open for 2% -> 0% of each run, Pallas kernels for 32% -> 0%
where the time goes in v2:
time: 87.8 us; the launch traced here: 87.7 us
  Pallas kernels  86.1 us (98%)
  local copies, waits for them, and re-layouts  1.57 us (2%)
    pallas_call x1, Pallas kernels, local(): pl.pallas_call(layer_kernel, out_shape=jax.ShapeDtypeStruct((TOK, COLS),...  86.1 us

profile of v2, /device:TPU:1, one launch (start us, length us, event | category | flops | bytes accessed | tf_op | source)
XLA Modules:
  0.0 87.7 jit_solution(10628309968379522014)
XLA Ops:
  0.0 86.1 %shard_map.127 = bf16[128,512]{1,0:T(8,128)(2,1)} custom-call(bf16[128,256]{1,0:T(8,128)(2,1)} %q_ref.1, bf16[128,256]{1,0:T(8,128)(2,1)} %k_ref.1, bf16[128,512]{1,0:T(8,128)(2,1)} %v_ref.1, bf16[128,512]{1,0:T(8,128)(2,1)} %og_ref.1, f32[2,128]{1,0:T(2,128)} %bitcast.8, f32[2,128]{1,0:T(2,128)} %bitcast.9, f32[1,512]{1,0:T(1,128)} %bitcast.7, ...), custom_call_target="tpu_custom_call" | custom-call | tf_op jit(solution)/shard_map/pallas_call | solution.py:568
  86.1 1.6 %copy.15 = bf16[128,512]{1,0:T(8,128)(2,1)} copy(bf16[128,512]{1,0:T(8,128)(2,1)} %shard_map.127) | data formatting | bytes 262144

commit v3 on v2

--- a/solution.py
+++ b/solution.py
@@ -58,14 +58,130 @@
     return bar, len(devs)
 
 
+COLUMNS = (0, -1, 1, -2, 2, -3, 3, 4)
+SPLIT = {"u": 512, "d": 640}
+STEPS = {
+    "first": (
+        ("own", "u"),
+        ("by", "u", 0),
+    ),
+    "slices": (
+        ("ayf", "u"),
+    ),
+    "totals": (
+        ("bz", "u", 1),
+        ("by", "u", 1),
+        ("by", "u", 2),
+        ("byf", "u", 0),
+        ("az", "u", 0),
+        ("own", "d"),
+        ("by", "d", 0),
+        ("byf", "u", 1),
+    ),
+    "prefix": (
+        ("bz", "u", 2),
+        ("by", "u", 3),
+        ("by", "u", 4),
+        ("byf", "u", 2),
+        ("sb", "u", 0),
+    ),
+    "parts": (
+        ("az", "u", 1),
+        ("sb", "u", 1),
+        ("ayf", "d"),
+        ("byf", "d", 0),
+        ("bz", "d", 1),
+        ("bz", "u", 3),
+        ("by", "u", 5),
+        ("by", "u", 6),
+        ("byf", "u", 3),
+        ("byf", "u", 4),
+        ("sb", "u", 2),
+        ("az", "d", 0),
+        ("sb", "d", 0),
+    ),
+    "feats": (
+        ("az", "u", 2),
+        ("by", "d", 1),
+        ("byf", "u", 5),
+        ("bz", "u", 4),
+        ("by", "u", 7),
+        ("byf", "u", 6),
+        ("sb", "u", 3),
+        ("bz", "d", 2),
+        ("sb", "u", 4),
+        ("az", "d", 1),
+        ("by", "d", 2),
+    ),
+    "rest": (
+        ("fa", "u", -2),
+        ("fa", "u", -1),
+        ("fb", "u", 0),
+        ("fa", "u", 0),
+        ("fb", "u", 1),
+        ("fa", "u", 1),
+        ("sb", "u", 5),
+        ("fb", "u", 2),
+        ("fa", "u", 2),
+        ("fb", "u", 3),
+        ("fb", "u", 4),
+        ("by", "d", 3),
+        ("by", "d", 4),
+        ("byf", "d", 1),
+        ("byf", "u", 7),
+        ("az", "u", 3),
+        ("fb", "u", 5),
+        ("sb", "u", 6),
+        ("bz", "d", 3),
+        ("by", "d", 5),
+        ("by", "d", 6),
+        ("fa", "u", -3),
+        ("byf", "d", 2),
+        ("fa", "u", 3),
+        ("byf", "d", 3),
+        ("fb", "u", 6),
+        ("byf", "d", 4),
+        ("az", "d", 2),
+        ("sb", "d", 1),
+        ("sb", "u", 7),
+        ("byf", "d", 5),
+        ("az", "u", 4),
+        ("bz", "d", 4),
+        ("by", "d", 7),
+        ("byf", "d", 6),
+        ("sb", "d", 2),
+        ("fb", "u", 7),
+        ("sb", "d", 3),
+        ("fa", "u", 4),
+        ("hid", "u"),
+        ("sb", "d", 4),
+        ("sb", "d", 5),
+        ("dn", "d", 0),
+        ("byf", "d", 7),
+        ("az", "d", 3),
+        ("sb", "d", 6),
+        ("dn", "d", 3),
+        ("sb", "d", 7),
+        ("dn", "d", 1),
+        ("az", "d", 4),
+        ("dn", "d", 2),
+    ),
+}
+
+
 class Weights:
     def __init__(self, w, wss, wrs, z, g, tp):
         self.w, self.wss, self.wrs = w, wss, wrs
         self.z, self.y, self.c, self.tp = z, g // 2, lax.rem(g, 2), tp
         self.ids, self.sent = {}, []
-        self.zi = [lax.rem(z + k, NZ) for k in (0, 7, 1, 6, 2, 5, 3, 4)]
-        z_at = lambda k: {"sp": lax.rem(z + k, NZ) * NG + g, "tp": tp}
-        y_at = lambda k: {"sp": z * NG + lax.rem(self.y + k, 4) * 2 + self.c, "tp": tp}
+        self.zi = [self.zk(k) for k in COLUMNS]
+
+        def z_at(k):
+            return {"sp": lax.rem(z + k, NZ) * NG + g, "tp": tp}
+
+        def y_at(k):
+            return {"sp": z * NG + lax.rem(self.y + k, 4) * 2 + self.c, "tp": tp}
+
         self.dev = {
             "z+": z_at(1),
             "z-": z_at(7),
@@ -80,8 +196,18 @@
     def yk(self, k):
         return lax.rem(self.y + 4 + k, 4)
 
-    def both(self, zi, yi):
-        return (pl.ds(0, 2), zi, yi, self.c)
+    def lanes(self, f, route):
+        cut = SPLIT[f]
+        return pl.ds(0, cut) if route == "a" else pl.ds(cut, FFT - cut)
+
+    def at(self, f, route, zi, yi, half=None, core=None):
+        lanes, rows = self.lanes(f, route), pl.ds(0, 32)
+        if f == "u":
+            kind = pl.ds(0, 2) if half is None else half
+        else:
+            kind = 2
+            rows = rows if half is None else pl.ds(16 * half, 16)
+        return (kind, zi, yi, self.c if core is None else core, rows, lanes)
 
     def desc(self, name, way, at):
         n = self.ids.setdefault((name, way), len(self.ids))
@@ -95,129 +221,76 @@
     def got(self, name, way, at):
         self.desc(name, way, at).wait_recv()
 
-    def first(self):
-        own = self.both(self.z, self.y)
-        self.send("bz1", "z+", own)
-        self.send("bz1", "z-", own)
-        down = (2, self.z, self.y, self.c)
-        self.send("ay", "y+", down)
-        self.send("ay", "y-", down)
-        self.by(0)
-
-    def bz(self, k):
+    def own(self, f):
+        for way in ("z+", "z-"):
+            self.send(f"bz{f}1", way, self.at(f, "b", self.z, self.y))
+        for way in ("y+", "y-"):
+            self.send(f"ay{f}", way, self.at(f, "a", self.z, self.y))
+
+    def bz(self, f, k):
         back, ahead = self.zk(-k), self.zk(k)
+        halves = (0, 1) if k == 4 else (None, None)
+        self.got(f"bz{f}{k}", "z+", self.at(f, "b", back, self.y, halves[0]))
+        self.got(f"bz{f}{k}", "z-", self.at(f, "b", ahead, self.y, halves[1]))
+        if k < 4:
+            halves = (0, 1) if k == 3 else (None, None)
+            self.send(f"bz{f}{k + 1}", "z+", self.at(f, "b", back, self.y, halves[0]))
+            self.send(f"bz{f}{k + 1}", "z-", self.at(f, "b", ahead, self.y, halves[1]))
+
+    def by(self, f, j):
+        for way in ("y+", "y-"):
+            self.send(f"by{f}{j}", way, self.at(f, "b", self.zi[j], self.y))
+
+    def byf(self, f, j):
+        for way, step, half in (("y+", -1, 0), ("y-", 1, 1)):
+            self.got(f"by{f}{j}", way, self.at(f, "b", self.zi[j], self.yk(step)))
+            self.send(f"byf{f}{j}", way, self.at(f, "b", self.zi[j], self.yk(step), half))
+
+    def sb(self, f, j):
+        for way, half in (("y+", 0), ("y-", 1)):
+            self.got(f"byf{f}{j}", way, self.at(f, "b", self.zi[j], self.yk(2), half))
+        self.send(f"sb{f}{j}", "s", self.at(f, "b", self.zi[j], pl.ds(0, 4)))
+
+    def ayf(self, f):
+        for way, step, half in (("y+", -1, 0), ("y-", 1, 1)):
+            self.got(f"ay{f}", way, self.at(f, "a", self.z, self.yk(step)))
+            self.send(f"ayf{f}", way, self.at(f, "a", self.z, self.yk(step), half))
+
+    def sa(self, f, k):
+        self.send(f"sa{f}{k}", "s", self.at(f, "a", self.zk(k), pl.ds(0, 4)))
+
+    def az(self, f, k):
+        if k == 0:
+            for way, half in (("y+", 0), ("y-", 1)):
+                self.got(f"ayf{f}", way, self.at(f, "a", self.z, self.yk(2), half))
+        ends = (("z+", self.zk(-k), 0), ("z-", self.zk(k), 1))
         if k == 4:
-            self.got("bz4", "z+", (0, back, self.y, self.c))
-            self.got("bz4", "z-", (1, ahead, self.y, self.c))
-            return
-        self.got(f"bz{k}", "z+", self.both(back, self.y))
-        self.got(f"bz{k}", "z-", self.both(ahead, self.y))
-        if k == 3:
-            self.send("bz4", "z+", (0, back, self.y, self.c))
-            self.send("bz4", "z-", (1, ahead, self.y, self.c))
-        else:
-            self.send(f"bz{k + 1}", "z+", self.both(back, self.y))
-            self.send(f"bz{k + 1}", "z-", self.both(ahead, self.y))
-
-    def by(self, j):
-        self.send(f"by{j}", "y+", self.both(self.zi[j], self.y))
-        self.send(f"by{j}", "y-", self.both(self.zi[j], self.y))
-
-    def byf(self, j):
-        self.got(f"by{j}", "y+", self.both(self.zi[j], self.yk(-1)))
-        self.send(f"byf{j}", "y+", (0, self.zi[j], self.yk(-1), self.c))
-        self.got(f"by{j}", "y-", self.both(self.zi[j], self.yk(1)))
-        self.send(f"byf{j}", "y-", (1, self.zi[j], self.yk(1), self.c))
-
-    def sb(self, j):
-        self.got(f"byf{j}", "y+", (0, self.zi[j], self.yk(-2), self.c))
-        self.got(f"byf{j}", "y-", (1, self.zi[j], self.yk(2), self.c))
-        self.send(f"sb{j}", "s", (pl.ds(0, 2), self.zi[j], pl.ds(0, 4), self.c))
-
-    def ayf(self):
-        self.got("ay", "y+", (2, self.z, self.yk(-1), self.c))
-        self.send("ayf", "y+", (2, self.z, self.yk(-1), self.c, pl.ds(0, 16)))
-        self.got("ay", "y-", (2, self.z, self.yk(1), self.c))
-        self.send("ayf", "y-", (2, self.z, self.yk(1), self.c, pl.ds(16, 16)))
-
-    def pair(self, zi, p):
-        return (2, zi, pl.ds(2 * p, 2), self.c)
-
-    def sa(self, k):
-        self.send(f"sa{k}", "s", (2, self.zk(k), pl.ds(0, 4), self.c))
-
-    def az(self, k):
-        if k == 0:
-            self.got("ayf", "y+", (2, self.z, self.yk(-2), self.c, pl.ds(0, 16)))
-            self.got("ayf", "y-", (2, self.z, self.yk(2), self.c, pl.ds(16, 16)))
-        back, ahead = self.zk(-k), self.zk(k)
-        if k == 4:
-            self.got("az4", "z+", self.pair(back, 0))
-            self.got("az4", "z-", self.pair(ahead, 1))
-            self.sa(4)
+            for way, zi, p in ends:
+                self.got(f"az{f}4", way, self.at(f, "a", zi, pl.ds(2 * p, 2)))
+            self.sa(f, 4)
             return
         for p in range(2):
-            if k:
-                self.got(f"az{k}{p}", "z+", self.pair(back, p))
-            if k < 3:
-                self.send(f"az{k + 1}{p}", "z+", self.pair(back, p))
-            elif p == 0:
-                self.send("az4", "z+", self.pair(back, 0))
-            if k:
-                self.got(f"az{k}{p}", "z-", self.pair(ahead, p))
-            if k < 3:
-                self.send(f"az{k + 1}{p}", "z-", self.pair(ahead, p))
-            elif p == 1:
-                self.send("az4", "z-", self.pair(ahead, 1))
-        self.sa(-k)
+            for way, zi, mine in ends:
+                at = self.at(f, "a", zi, pl.ds(2 * p, 2))
+                if k:
+                    self.got(f"az{f}{k}{p}", way, at)
+                if k < 3:
+                    self.send(f"az{f}{k + 1}{p}", way, at)
+                elif p == mine:
+                    self.send(f"az{f}4", way, at)
+        self.sa(f, -k)
         if k:
-            self.sa(k)
-
-    def after_slices(self):
-        self.bz(1)
-        self.ayf()
-        self.byf(0)
-        self.by(1)
-        self.by(2)
-
-    def after_totals(self):
-        self.bz(2)
-        self.az(0)
-
-    def after_prefixes(self):
-        self.bz(3)
-        for j in (3, 4, 5, 6):
-            self.by(j)
-        self.byf(1)
-        self.byf(2)
-
-    def after_partials(self):
-        self.bz(4)
-        self.by(7)
-        self.az(1)
-        self.sb(0)
-
-    def after_features(self):
-        self.az(2)
-        for j in (1, 2):
-            self.sb(j)
-        for j in (3, 4):
-            self.byf(j)
-
-    def before_column(self, j):
-        if j == 0:
-            self.az(3)
-            for k in (5, 6, 7):
-                self.byf(k)
-        if j >= 3:
-            self.sb(j)
-        if j == 5:
-            self.az(4)
-        self.got(f"sb{j}", "s", (pl.ds(0, 2), self.zi[j], pl.ds(0, 4), 1 - self.c))
-
-    def before_down(self):
-        for k in (0, -1, 1, -2, 2, -3, 3, 4):
-            self.got(f"sa{k}", "s", (2, self.zk(k), pl.ds(0, 4), 1 - self.c))
+            self.sa(f, k)
+
+    def column_b(self, f, j):
+        self.got(f"sb{f}{j}", "s", self.at(f, "b", self.zi[j], pl.ds(0, 4), core=1 - self.c))
+
+    def column_a(self, f, k):
+        self.got(f"sa{f}{k}", "s", self.at(f, "a", self.zk(k), pl.ds(0, 4), core=1 - self.c))
+
+    def slot(self, name):
+        for kind, *rest in STEPS[name]:
+            getattr(self, kind)(*rest)
 
 
 def layer_kernel(
@@ -238,6 +311,7 @@
     w,
     wo,
     acc,
+    hid,
     y_ref,
     small1,
     small2,
@@ -319,7 +393,7 @@
     small1[g] = small_me[...]
     for c in loads[:3]:
         c.wait()
-    net.first()
+    net.slot("first")
 
     for h in range(2):
         hi, lo = split_hi_lo(wks[h])
@@ -331,7 +405,7 @@
         c.start()
         pending.append(c)
     r1[g] = s_loc[g]
-    net.after_slices()
+    net.slot("slices")
 
     scale = DQK**-0.5
     num0, den0, peak0 = [], [], []
@@ -398,7 +472,7 @@
         c.start()
         pending.append(c)
     r2[z] = t_loc[...]
-    net.after_totals()
+    net.slot("totals")
 
     for r in range(1, NZ):
         copy_to(
@@ -452,7 +526,7 @@
         c.start()
         pending.append(c)
     r3[g] = o3[g]
-    net.after_prefixes()
+    net.slot("prefix")
     gates = [
         hg_ref[:, h * DV : (h + 1) * DV]
         / (1.0 + jnp.exp(-og_ref[:, h * DV : (h + 1) * DV].astype(f32)))
@@ -483,7 +557,7 @@
             c.start()
             pending.append(c)
     rpart[tp] = part[tp]
-    net.after_partials()
+    net.slot("parts")
     for r in range(1, NX):
         copy_to(sq_me.at[0], rsq.at[0, xfrom[r]], ss.at[5, r], rs.at[5, r], xdev[r]).wait_recv()
     sq_all = jnp.sum(rsq[0, :, 0, :], axis=0, keepdims=True)
@@ -510,40 +584,63 @@
         pending.append(c)
     rsq[1, tp] = sq_me[1]
     y_ref[tp] = yloc[...]
-    net.after_features()
+    net.slot("feats")
     for r in range(1, NX):
         copy_to(sq_me.at[1], rsq.at[1, xfrom[r]], ss.at[7, r], rs.at[7, r], xdev[r]).wait_recv()
     sq_all = jnp.sum(rsq[1, :, 0, :], axis=0, keepdims=True)
     scale_in = col_of(lax.rsqrt(sq_all / D + norm_eps), eye)
     for r in range(1, NX):
         copy_to(yloc, y_ref.at[xfrom[r]], ss.at[8, r], rs.at[8, r], xdev[r]).wait_recv()
-    for j in range(NZ):
-        net.before_column(j)
-        zi = net.zi[j]
-        y_col = y_ref[zi // 2, :, pl.ds(pl.multiple_of(lax.rem(zi, 2) * 256, 256), 256)]
+    def y_col(zi):
+        return y_ref[zi // 2, :, pl.ds(pl.multiple_of(lax.rem(zi, 2) * 256, 256), 256)]
+
+    seen = set()
+
+    def column(route, zi):
+        lanes = net.lanes("u", route)
         for kind in range(2):
-            term = dot(y_col, w[kind, zi].reshape(256, FFT))
-            if j == 0:
-                acc[kind] = term
+            term = dot(y_col(zi), w[kind, zi, :, :, :, lanes].reshape(256, lanes.size))
+            if (route, kind) in seen:
+                acc[kind, :, lanes] += term
             else:
-                acc[kind] += term
-    gate = acc[0] * scale_in
-    hidden = (gate / (1.0 + jnp.exp(-gate)) * (acc[1] * scale_in)).astype(bf16)
-    net.before_down()
-    for r in (2, 1, 3, 0):
-        at = xpeer[r]
-        part2[at] = dot(
-            hidden, w[2, pl.ds(2 * at, 2)].reshape(COLS, FFT), ((1,), (1,))
-        ).astype(bf16)
-        if r:
-            c = copy_to(part2.at[at], rpart2.at[tp], ss.at[9, r], rs.at[9, r], xdev[r])
-            c.start()
-            pending.append(c)
+                acc[kind, :, lanes] = term
+            seen.add((route, kind))
+
+    arrived = set()
+    for kind, *rest in STEPS["rest"]:
+        if kind == "fb":
+            net.column_b(*rest)
+            column("b", net.zi[rest[1]])
+        elif kind == "fa":
+            net.column_a(*rest)
+            column("a", net.zk(rest[1]))
+        elif kind == "hid":
+            gate = acc[0] * scale_in
+            hid[...] = (gate / (1.0 + jnp.exp(-gate)) * (acc[1] * scale_in)).astype(bf16)
+        elif kind == "dn":
+            for k in {0: (0, -1, 1), 1: (2, 3), 3: (-2, -3), 2: (4,)}[rest[1]]:
+                net.column_b("d", COLUMNS.index(k))
+                net.column_a("d", k)
+            at = lax.rem(z // 2 + rest[1], NX)
+            part2[at] = dot(
+                hid[...], w[2, pl.ds(2 * at, 2)].reshape(COLS, FFT), ((1,), (1,))
+            ).astype(bf16)
+
+            @pl.when(at != tp)
+            def _():
+                r = lax.rem(at - tp + NX, NX)
+                copy_to(
+                    part2.at[at], rpart2.at[tp], ss.at[9, r], rs.at[9, r], {"sp": sp, "tp": at}
+                ).start()
+        else:
+            getattr(net, kind)(*rest)
     total = resid_f + part2[tp].astype(f32)
-    for r in (1, 3, 2):
+    for r in range(1, NX):
         copy_to(part2.at[0], rpart2.at[xfrom[r]], ss.at[9, r], rs.at[9, r], xdev[r]).wait_recv()
         total = total + rpart2[xfrom[r]].astype(f32)
     o_ref[...] = total.astype(bf16)
+    for r in range(1, NX):
+        copy_to(part2.at[0], rpart2.at[tp], ss.at[9, r], rs.at[9, r], xdev[r]).wait_send()
     for c in pending + net.sent:
         c.wait_send()
 
@@ -574,6 +671,7 @@
             pltpu.VMEM((3, NZ, 4, 2, 32, FFT), bf16),
             pltpu.VMEM((COLS, D), bf16),
             pltpu.VMEM((2, TOK, FFT), f32),
+            pltpu.VMEM((TOK, FFT), bf16),
             pltpu.VMEM((NX, TOK, COLS), bf16),
             pltpu.VMEM((NG, 8, TOK), f32),
             pltpu.VMEM((NZ, 8, TOK), f32),
@@ -597,8 +695,8 @@
             pltpu.SemaphoreType.DMA((4,)),
             pltpu.SemaphoreType.DMA((10, 8)),
             pltpu.SemaphoreType.DMA((10, 8)),
-            pltpu.SemaphoreType.DMA((96,)),
-            pltpu.SemaphoreType.DMA((96,)),
+            pltpu.SemaphoreType.DMA((160,)),
+            pltpu.SemaphoreType.DMA((160,)),
         ],
         compiler_params=pltpu.CompilerParams(
             collective_id=0, has_side_effects=True, vmem_limit_bytes=60 * 2**20

time: 87.8 us -> 83.9 us (0.956)
  the two profiles are of different devices: /device:TPU:1 before, /device:TPU:5 now
where the time goes in v3:
time: 83.9 us; the launch traced here: 83.8 us
  Pallas kernels  82.2 us (98%)
  local copies, waits for them, and re-layouts  1.57 us (2%)
    pallas_call x1, Pallas kernels, local(): pl.pallas_call(layer_kernel, out_shape=jax.ShapeDtypeStruct((TOK, COLS),...  82.2 us

profile of v3, /device:TPU:5, one launch (start us, length us, event | category | flops | bytes accessed | tf_op | source)
XLA Modules:
  0.0 83.8 jit_solution(11180684339320726534)
XLA Ops:
  0.0 82.2 %shard_map.127 = bf16[128,512]{1,0:T(8,128)(2,1)} custom-call(bf16[128,256]{1,0:T(8,128)(2,1)} %q_ref.1, bf16[128,256]{1,0:T(8,128)(2,1)} %k_ref.1, bf16[128,512]{1,0:T(8,128)(2,1)} %v_ref.1, bf16[128,512]{1,0:T(8,128)(2,1)} %og_ref.1, f32[2,128]{1,0:T(2,128)} %bitcast.8, f32[2,128]{1,0:T(2,128)} %bitcast.9, f32[1,512]{1,0:T(1,128)} %bitcast.7, ...), custom_call_target="tpu_custom_call" | custom-call | tf_op jit(solution)/shard_map/pallas_call | solution.py:665
  82.2 1.6 %copy.15 = bf16[128,512]{1,0:T(8,128)(2,1)} copy(bf16[128,512]{1,0:T(8,128)(2,1)} %shard_map.127) | data formatting | bytes 262144

commit v4 on v3

v4 whole, which is shorter than its diff:
```python
import functools

import jax
import jax.numpy as jnp
from jax import lax
from jax.experimental import pallas as pl
from jax.experimental.pallas import tpu as pltpu
from jax.sharding import PartitionSpec as P

D = 2048
DQK = 128
DV = 256
VALS = 2048
FFT = 1408
TOK = 128
COLS = 512
NG = 8
NZ = 8
NX = 4
norm_eps = 1e-06
very_low = -1e30
MESH = pl.DeviceIdType.MESH
f32 = jnp.float32
bf16 = jnp.bfloat16


def row_of(col, eye):
    return jnp.sum(jnp.where(eye, col, 0.0), axis=0, keepdims=True)


def col_of(row, eye):
    return jnp.sum(jnp.where(eye, row, 0.0), axis=1, keepdims=True)


def split_hi_lo(x):
    hi = x.astype(bf16)
    return hi, (x - hi.astype(f32)).astype(bf16)


def dot(a, b, dims=((1,), (0,))):
    return lax.dot_general(a, b, (dims, ((), ())), preferred_element_type=f32)


def log_sigmoid(x):
    return jnp.minimum(x, 0.0) - jnp.log1p(jnp.exp(-jnp.abs(x)))


def copy_to(src, dst, ssem, rsem, dev):
    return pltpu.make_async_remote_copy(
        src_ref=src, dst_ref=dst, send_sem=ssem, recv_sem=rsem, device_id=dev, device_id_type=MESH
    )


def barrier_all(devs):
    bar = pltpu.get_barrier_semaphore()
    for dev in devs:
        pl.semaphore_signal(bar, inc=1, device_id=dev, device_id_type=MESH)
    return bar, len(devs)


RING = 6
COLUMNS = (0, -1, 1, -2, 2, -3, 3, 4)
GROUPS = {0: (0, -1, 1), 1: (2, 3), 3: (-2, -3), 2: (4,)}
GROUP_OF = {k: m for m, ks in GROUPS.items() for k in ks}
SPLIT = {"u": 512, "d": 640}
STEPS = {
    "first": (
        ("own", "u"),
        ("by", "u", 0),
    ),
    "slices": (
    ),
    "totals": (
        ("ayf", "u"),
        ("bz", "u", 1),
        ("by", "u", 1),
        ("by", "u", 2),
        ("byf", "u", 0),
        ("az", "u", 0),
        ("sa", "u", 0),
        ("byf", "u", 1),
    ),
    "prefix": (
        ("own", "d"),
        ("bz", "u", 2),
        ("by", "u", 3),
        ("by", "u", 4),
        ("byf", "u", 2),
        ("sb", "u", 0),
        ("sb", "u", 1),
    ),
    "parts": (
        ("az", "u", 1),
        ("sa", "u", -1),
        ("sa", "u", 1),
        ("ayf", "d"),
        ("byf", "u", 3),
        ("bz", "d", 1),
        ("bz", "u", 3),
        ("by", "u", 5),
        ("by", "u", 6),
        ("byf", "u", 4),
        ("sb", "u", 2),
        ("az", "d", 0),
        ("sa", "d", 0),
        ("sb", "u", 3),
        ("az", "u", 2),
        ("sa", "u", -2),
    ),
    "feats": (
        ("sa", "u", 2),
        ("by", "d", 0),
        ("byf", "u", 5),
        ("bz", "u", 4),
        ("by", "u", 7),
        ("byf", "u", 6),
        ("sb", "u", 4),
        ("bz", "d", 2),
        ("az", "d", 1),
        ("sa", "d", -1),
        ("sa", "d", 1),
        ("by", "d", 1),
        ("sb", "u", 5),
    ),
    "rest": (
        ("fa", "u", -2),
        ("fa", "u", -1),
        ("fb", "u", 0),
        ("fa", "u", 0),
        ("fb", "u", 1),
        ("fa", "u", 1),
        ("fb", "u", 2),
        ("fa", "u", 2),
        ("fb", "u", 3),
        ("byf", "u", 7),
        ("fb", "u", 4),
        ("fb", "u", 5),
        ("by", "d", 2),
        ("by", "d", 3),
        ("sb", "u", 6),
        ("by", "d", 4),
        ("az", "u", 3),
        ("sa", "u", -3),
        ("sa", "u", 3),
        ("byf", "d", 0),
        ("byf", "d", 1),
        ("bz", "d", 3),
        ("fb", "u", 6),
        ("sb", "u", 7),
        ("by", "d", 5),
        ("fa", "u", -3),
        ("by", "d", 6),
        ("fa", "u", 3),
        ("byf", "d", 2),
        ("fb", "u", 7),
        ("az", "d", 2),
        ("byf", "d", 3),
        ("sa", "d", -2),
        ("sa", "d", 2),
        ("byf", "d", 4),
        ("sb", "d", 0),
        ("sb", "d", 1),
        ("byf", "d", 5),
        ("az", "u", 4),
        ("sa", "u", 4),
        ("bz", "d", 4),
        ("by", "d", 7),
        ("byf", "d", 6),
        ("sb", "d", 2),
        ("sb", "d", 3),
        ("fa", "u", 4),
        ("hid", "u"),
        ("sb", "d", 4),
        ("dn", "d", 0),
        ("sb", "d", 5),
        ("byf", "d", 7),
        ("az", "d", 3),
        ("sa", "d", -3),
        ("sa", "d", 3),
        ("sb", "d", 6),
        ("dn", "d", 3),
        ("sb", "d", 7),
        ("dn", "d", 1),
        ("az", "d", 4),
        ("sa", "d", 4),
        ("dn", "d", 2),
    ),
}


class Weights:
    def __init__(self, bufs, ssem, rsem, z, g, tp):
        self.bufs, self.ssem, self.rsem = bufs, ssem, rsem
        self.z, self.y, self.c, self.tp = z, g // 2, lax.rem(g, 2), tp
        self.ids, self.sent = {}, {}
        self.zi = [self.zk(k) for k in COLUMNS]

        def z_at(k):
            return {"sp": lax.rem(z + k, NZ) * NG + g, "tp": tp}

        def y_at(k):
            return {"sp": z * NG + lax.rem(self.y + k, 4) * 2 + self.c, "tp": tp}

        self.dev = {
            "z+": z_at(1),
            "z-": z_at(7),
            "y+": y_at(1),
            "y-": y_at(3),
            "s": {"sp": z * NG + self.y * 2 + (1 - self.c), "tp": tp},
        }
        self.ways = list(self.dev)

    def zk(self, k):
        return lax.rem(self.z + NZ + k, NZ)

    def yk(self, k):
        return lax.rem(self.y + 4 + k, 4)

    def at(self, f, route, zi, yi, half=None, core=None):
        kinds, rows = pl.ds(0, 2 if f == "u" else 1), pl.ds(0, 32)
        if half is not None:
            kinds, rows = (pl.ds(half, 1), rows) if f == "u" else (kinds, pl.ds(16 * half, 16))
        zs = zi if isinstance(zi, pl.Slice) else pl.ds(zi, 1)
        ys = yi if isinstance(yi, pl.Slice) else pl.ds(yi, 1)
        return self.bufs[f, route].at[kinds, zs, self.c if core is None else core, ys, rows]

    def send(self, name, way, ref):
        n = self.ids.setdefault(name, len(self.ids))
        past = self.sent.setdefault(way, [])
        k = len(past)
        if k >= RING:
            past[k - RING].wait_send()
        slot = self.ways.index(way) * RING + k % RING
        c = copy_to(ref, ref, self.ssem.at[slot], self.rsem.at[n], self.dev[way])
        c.start()
        past.append(c)

    def got(self, name, ref):
        n = self.ids.setdefault(name, len(self.ids))
        copy_to(ref, ref, self.ssem.at[0], self.rsem.at[n], self.dev["s"]).wait_recv()

    def drain(self):
        for past in self.sent.values():
            for c in past[-RING:]:
                c.wait_send()

    def own(self, f):
        for way in ("z+", "z-"):
            self.send(f"bz{f}1", way, self.at(f, "b", self.z, self.y))
        for way in ("y+", "y-"):
            self.send(f"ay{f}", way, self.at(f, "a", self.z, self.y))

    def bz(self, f, k):
        self.got(f"bz{f}{k}", self.at(f, "b", pl.ds(0, 1 if k == 4 else 2), self.y))
        if k < 4:
            halves = (0, 1) if k == 3 else (None, None)
            self.send(f"bz{f}{k + 1}", "z+", self.at(f, "b", self.zk(-k), self.y, halves[0]))
            self.send(f"bz{f}{k + 1}", "z-", self.at(f, "b", self.zk(k), self.y, halves[1]))

    def by(self, f, j):
        for way in ("y+", "y-"):
            self.send(f"by{f}{j}", way, self.at(f, "b", self.zi[j], self.y))

    def byf(self, f, j):
        self.got(f"by{f}{j}", self.at(f, "b", self.zi[j], pl.ds(0, 2)))
        self.send(f"byf{f}{j}", "y+", self.at(f, "b", self.zi[j], self.yk(-1), 0))
        self.send(f"byf{f}{j}", "y-", self.at(f, "b", self.zi[j], self.yk(1), 1))

    def sb(self, f, j):
        self.got(f"byf{f}{j}", self.at(f, "b", self.zi[j], self.yk(2)))
        group = j if f == "u" else GROUP_OF[COLUMNS[j]]
        self.send(f"sb{f}{group}", "s", self.at(f, "b", self.zi[j], pl.ds(0, 4)))

    def ayf(self, f):
        self.got(f"ay{f}", self.at(f, "a", self.z, pl.ds(0, 2)))
        self.send(f"ayf{f}", "y+", self.at(f, "a", self.z, self.yk(-1), 0))
        self.send(f"ayf{f}", "y-", self.at(f, "a", self.z, self.yk(1), 1))

    def sa(self, f, k):
        group = k if f == "u" else GROUP_OF[k]
        self.send(f"sa{f}{group}", "s", self.at(f, "a", self.zk(k), pl.ds(0, 4)))

    def az(self, f, k):
        if k == 0:
            self.got(f"ayf{f}", self.at(f, "a", self.z, self.yk(2)))
        else:
            self.got(f"az{f}{k}", self.at(f, "a", pl.ds(0, 1 if k == 4 else 2), pl.ds(0, 4)))
        if k == 4:
            return
        for p in range(2):
            for way, zi, mine in (("z+", self.zk(-k), 0), ("z-", self.zk(k), 1)):
                if k < 3 or p == mine:
                    self.send(f"az{f}{k + 1}", way, self.at(f, "a", zi, pl.ds(2 * p, 2)))

    def column_b(self, j):
        self.got(f"sbu{j}", self.at("u", "b", self.zi[j], pl.ds(0, 4)))

    def column_a(self, k):
        self.got(f"sau{k}", self.at("u", "a", self.zk(k), pl.ds(0, 4)))

    def columns_down(self, m):
        for route in "ab":
            self.got(f"s{route}d{m}", self.at("d", route, pl.ds(0, len(GROUPS[m])), pl.ds(0, 4)))

    def slot(self, name):
        for kind, *rest in STEPS[name]:
            getattr(self, kind)(*rest)


def layer_kernel(
    q_ref,
    k_ref,
    v_ref,
    og_ref,
    ig_ref,
    fg_ref,
    hg_ref,
    wo_hbm,
    st_ref,
    gain_ref,
    wg_hbm,
    wu_hbm,
    wd_hbm,
    o_ref,
    ua,
    ub,
    da,
    db,
    wo,
    acc,
    hid,
    y_ref,
    small1,
    small2,
    small_l,
    small_me,
    small_t,
    s_loc,
    r1,
    pre_l,
    t_loc,
    r2,
    o3,
    r3,
    part,
    rpart,
    sq_me,
    rsq,
    yloc,
    part2,
    rpart2,
    lsem,
    ss,
    rs,
    wss,
    wrs,
):
    sp, tp = lax.axis_index("sp"), lax.axis_index("tp")
    z, g = sp // NG, lax.rem(sp, NG)
    gpeer = [lax.rem(g + r, NG) for r in range(NG)]
    gfrom = [lax.rem(g + NG - r, NG) for r in range(NG)]
    zpeer = [lax.rem(z + r, NZ) for r in range(NZ)]
    xpeer = [lax.rem(tp + r, NX) for r in range(NX)]
    xfrom = [lax.rem(tp + NX - r, NX) for r in range(NX)]
    gdev = [{"sp": z * NG + p, "tp": tp} for p in gpeer]
    zdev = [{"sp": p * NG + g, "tp": tp} for p in zpeer]
    xdev = [{"sp": sp, "tp": p} for p in xpeer]
    def joint(n, ref):
        return copy_to(ref, ref, ss.at[n], rs.at[n], gdev[1])

    bar, count = barrier_all(gdev[1:] + zdev[1:] + xdev[1:])
    bufs = {("u", "a"): ua, ("u", "b"): ub, ("d", "a"): da, ("d", "b"): db}
    net = Weights(bufs, wss, wrs, z, g, tp)
    loads = []
    for f, kind, ref in (("u", 0, wg_hbm), ("u", 1, wu_hbm), ("d", 0, wd_hbm)):
        cut = SPLIT[f]
        for route, lanes in (("a", pl.ds(0, cut)), ("b", pl.ds(cut, FFT - cut))):
            loads.append(
                pltpu.make_async_copy(
                    ref.at[:, lanes], bufs[f, route].at[kind, z, net.c, net.y], lsem.at[len(loads)]
                )
            )
    loads.append(pltpu.make_async_copy(wo_hbm, wo, lsem.at[6]))
    for c in loads:
        c.start()
    rows = lax.broadcasted_iota(jnp.int32, (TOK, TOK), 0)
    cols = lax.broadcasted_iota(jnp.int32, (TOK, TOK), 1)
    eye = rows == cols
    low = rows >= cols

    lf = log_sigmoid(fg_ref[...])
    ig = ig_ref[...]
    small_me[...] = jnp.zeros_like(small_me)
    cs_cols, pairs, wks = [], [], []
    for h in range(2):
        lf_row = lf[h : h + 1, :]
        lf_col = col_of(lf_row, eye)
        cs_col = jnp.sum(jnp.where(low, lf_row, 0.0), axis=1, keepdims=True)
        cs_row = jnp.sum(jnp.where(rows <= cols, lf_col, 0.0), axis=0, keepdims=True)
        ig_row = ig[h : h + 1, :]
        rest_row = ig_row - cs_row
        rest_col = col_of(rest_row, eye)
        top = jnp.max(rest_row, axis=1, keepdims=True)
        total = jnp.sum(lf_row, axis=1, keepdims=True)
        wk = jnp.exp(rest_col - top) * k_ref[:, h * DQK : (h + 1) * DQK].astype(f32)
        small_me[h : h + 1, :] = jnp.sum(wk, axis=0, keepdims=True)
        small_me[2 + h : 3 + h, :] = jnp.broadcast_to(total, (1, TOK))
        small_me[4 + h : 5 + h, :] = jnp.broadcast_to(total + top, (1, TOK))
        cs_cols.append(cs_col)
        pairs.append((rest_row, ig_row))
        wks.append(wk)
    for h in range(2):
        hi, lo = split_hi_lo(wks[h])
        v_h = v_ref[:, h * DV : (h + 1) * DV]
        state = dot(hi, v_h, ((0,), (0,))) + dot(lo, v_h, ((0,), (0,)))
        s_loc[4 * h : 4 * h + 4] = state.astype(bf16).reshape(4, 32, DV)
    scale = DQK**-0.5
    num0, den0, peak0 = [], [], []
    for h in range(2):
        rest_row, ig_row = pairs[h]
        q_h = q_ref[:, h * DQK : (h + 1) * DQK]
        k_h = k_ref[:, h * DQK : (h + 1) * DQK]
        log_pair = jnp.where(low, cs_cols[h] + rest_row, -jnp.inf)
        peak = jnp.max(log_pair, axis=1, keepdims=True)
        scores = dot(q_h, k_h, ((1,), (1,))) * scale * jnp.exp(log_pair - peak)
        hi, lo = split_hi_lo(scores)
        v_h = v_ref[:, h * DV : (h + 1) * DV]
        num0.append(dot(hi, v_h) + dot(lo, v_h))
        den0.append(jnp.sum(scores, axis=1, keepdims=True))
        peak0.append(peak)

    pl.semaphore_wait(bar, count)
    for r in range(1, NG):
        copy_to(small_me, small1.at[g], ss.at[0], rs.at[0], gdev[r]).start()
        copy_to(s_loc.at[gpeer[r]], r1.at[g], ss.at[1], rs.at[1], gdev[r]).start()
    for c in loads[:6]:
        c.wait()
    net.slot("first")
    small1[g] = small_me[...]
    r1[g] = s_loc[g]
    net.slot("slices")
    joint(0, small1.at[pl.ds(0, NG - 1)]).wait_recv()
    n_l = jnp.zeros((2, TOK), f32)
    a_l = jnp.zeros((2, TOK), f32)
    m_l = jnp.full((2, TOK), very_low, f32)
    a_list, m_list, f_list, l_list = [], [], [], []
    for i in range(NG):
        small_l[i, 0:2, :] = n_l
        small_l[i, 2:4, :] = a_l
        small_l[i, 4:6, :] = m_l
        a_list.append(a_l)
        m_list.append(m_l)
        n_i, a_i, m_i = small1[i, 0:2, :], small1[i, 2:4, :], small1[i, 4:6, :]
        new = jnp.maximum(a_i + m_l, m_i)
        former, latter = jnp.exp(a_i + m_l - new), jnp.exp(m_i - new)
        f_list.append(former)
        l_list.append(latter)
        n_l = former * n_l + latter * n_i
        a_l = a_l + a_i
        m_l = new
    small_t[...] = jnp.zeros_like(small_t)
    small_t[0:2, :] = n_l
    small_t[2:4, :] = a_l
    small_t[4:6, :] = m_l
    for r in range(1, NZ):
        copy_to(small_t, small2.at[z], ss.at[2], rs.at[2], zdev[r]).start()
    small2[z] = small_t[...]

    def mine(pair):
        return jnp.where(g < 4, pair[0:1, :], pair[1:2, :])

    def spread(line):
        return jnp.concatenate([line, line], axis=1)

    joint(1, r1.at[pl.ds(0, NG - 1)]).wait_recv()
    run = jnp.zeros((32, DV), f32)
    for i in range(NG):
        pre_l[i] = run
        run = spread(mine(f_list[i])) * run + spread(mine(l_list[i])) * r1[i].astype(f32)
    t_loc[...] = run.astype(bf16)
    for r in range(1, NZ):
        copy_to(t_loc, r2.at[z], ss.at[3], rs.at[3], zdev[r]).start()
    r2[z] = t_loc[...]
    net.slot("totals")

    joint(2, small2.at[pl.ds(0, NZ - 1)]).wait_recv()
    n_z = jnp.zeros((2, TOK), f32)
    m_z = jnp.full((2, TOK), very_low, f32)
    fz, lz = [], []
    for i in range(NZ):
        on = i < z
        n_i, a_i, m_i = small2[i, 0:2, :], small2[i, 2:4, :], small2[i, 4:6, :]
        new = jnp.maximum(a_i + m_z, m_i)
        former, latter = jnp.exp(a_i + m_z - new), jnp.exp(m_i - new)
        former = jnp.where(on, former, 1.0)
        latter = jnp.where(on, latter, 0.0)
        fz.append(mine(former))
        lz.append(mine(latter))
        n_z = former * n_z + latter * n_i
        m_z = jnp.where(on, new, m_z)
    ca, cb = [], []
    for j in range(NG):
        new = jnp.maximum(a_list[j] + m_z, m_list[j])
        ca.append(mine(jnp.exp(m_list[j] - new)))
        cb.append(mine(jnp.exp(a_list[j] + m_z - new)))
    n_g, a_g, m_g = small_l[g, 0:2, :], small_l[g, 2:4, :], small_l[g, 4:6, :]
    m_in = jnp.maximum(a_g + m_z, m_g)
    n_in = jnp.exp(m_g - m_in) * n_g + jnp.exp(a_g + m_z - m_in) * n_z

    scale0, carried, denom = [], [], []
    for h in range(2):
        q_h = q_ref[:, h * DQK : (h + 1) * DQK].astype(f32)
        log_carry = cs_cols[h] + m_in[h : h + 1, 0:1]
        peak = jnp.maximum(peak0[h], log_carry)
        s0, c0 = jnp.exp(peak0[h] - peak), jnp.exp(log_carry - peak) * scale
        normer = s0 * den0[h] + c0 * jnp.sum(q_h * n_in[h : h + 1, :], axis=1, keepdims=True)
        inv = 1.0 / jnp.maximum(jnp.abs(normer), jnp.exp(-peak))
        scale0.append(s0 * inv)
        carried.append(c0 * inv)

    joint(3, r2.at[pl.ds(0, NZ - 1)]).wait_recv()
    run = jnp.zeros((32, DV), f32)
    for i in range(NZ):
        run = spread(fz[i]) * run + spread(lz[i]) * r2[i].astype(f32)
    for j in range(NG):
        o3[j] = (spread(ca[j]) * pre_l[j] + spread(cb[j]) * run).astype(bf16)
    for r in range(1, NG):
        copy_to(o3.at[gpeer[r]], r3.at[g], ss.at[4], rs.at[4], gdev[r]).start()
    r3[g] = o3[g]
    net.slot("prefix")
    gates = [
        hg_ref[:, h * DV : (h + 1) * DV]
        / (1.0 + jnp.exp(-og_ref[:, h * DV : (h + 1) * DV].astype(f32)))
        for h in range(2)
    ]
    joint(4, r3.at[pl.ds(0, NG - 1)]).wait_recv()
    gated, sq = [], jnp.zeros((TOK, 1), f32)
    for h in range(2):
        q_h = q_ref[:, h * DQK : (h + 1) * DQK]
        state = r3[4 * h : 4 * h + 4].reshape(DQK, DV)
        out = scale0[h] * num0[h] + carried[h] * dot(q_h, state)
        sq = sq + jnp.sum(out * out, axis=1, keepdims=True)
        gated.append((out * gates[h]).astype(bf16))
    sq_me[0] = jnp.broadcast_to(row_of(sq, eye), (8, TOK))
    for r in range(1, NX):
        copy_to(sq_me.at[0], rsq.at[0, tp], ss.at[5], rs.at[5], xdev[r]).start()
    rsq[0, tp] = sq_me[0]
    heads = jnp.concatenate(gated, axis=1)
    loads[6].wait()
    for r in (2, 1, 3, 0):
        at = pl.multiple_of(xpeer[r] * COLS, COLS)
        part[xpeer[r]] = dot(heads, wo[:, pl.ds(at, COLS)]).astype(bf16)
        if r:
            copy_to(part.at[xpeer[r]], rpart.at[tp], ss.at[6], rs.at[6], xdev[r]).start()
    rpart[tp] = part[tp]
    net.slot("parts")
    joint(5, rsq.at[0, pl.ds(0, NX - 1)]).wait_recv()
    sq_all = jnp.sum(rsq[0, :, 0, :], axis=0, keepdims=True)
    row_scale = col_of(lax.rsqrt(sq_all / VALS + norm_eps), eye)
    joint(6, rpart.at[pl.ds(0, NX - 1)]).wait_recv()
    mixer = rpart[0].astype(f32)
    for i in range(1, NX):
        mixer = mixer + rpart[i].astype(f32)
    resid = (st_ref[...].astype(f32) + mixer * row_scale).astype(bf16)
    resid_f = resid.astype(f32)
    gain = gain_ref[:, pl.ds(pl.multiple_of(tp * COLS, COLS), COLS)]
    yloc[...] = (resid_f * gain).astype(bf16)
    sq_me[1] = jnp.broadcast_to(
        row_of(jnp.sum(resid_f * resid_f, axis=1, keepdims=True), eye), (8, TOK)
    )
    for r in (2, 1, 3):
        copy_to(yloc, y_ref.at[tp], ss.at[8], rs.at[8], xdev[r]).start()
    for r in range(1, NX):
        copy_to(sq_me.at[1], rsq.at[1, tp], ss.at[7], rs.at[7], xdev[r]).start()
    rsq[1, tp] = sq_me[1]
    y_ref[tp] = yloc[...]
    net.slot("feats")
    joint(7, rsq.at[1, pl.ds(0, NX - 1)]).wait_recv()
    sq_all = jnp.sum(rsq[1, :, 0, :], axis=0, keepdims=True)
    scale_in = col_of(lax.rsqrt(sq_all / D + norm_eps), eye)
    joint(8, y_ref.at[pl.ds(0, NX - 1)]).wait_recv()
    def y_col(zi):
        return y_ref[zi // 2, :, pl.ds(pl.multiple_of(lax.rem(zi, 2) * 256, 256), 256)]

    seen = set()

    def rows_of(f, route, kind, zi):
        buf = bufs[f, route]
        return [buf[kind, zi, core, yi] for yi in range(4) for core in range(2)]

    def column(route, zi):
        cut = SPLIT["u"]
        lanes = pl.ds(0, cut) if route == "a" else pl.ds(cut, FFT - cut)
        for kind in range(2):
            term = dot(y_col(zi), jnp.concatenate(rows_of("u", route, kind, zi), axis=0))
            if (route, kind) in seen:
                acc[kind, :, lanes] += term
            else:
                acc[kind, :, lanes] = term
            seen.add((route, kind))

    for kind, *rest in STEPS["rest"]:
        if kind == "fb":
            net.column_b(rest[1])
            column("b", net.zi[rest[1]])
        elif kind == "fa":
            net.column_a(rest[1])
            column("a", net.zk(rest[1]))
        elif kind == "hid":
            gate = acc[0] * scale_in
            hid[...] = (gate / (1.0 + jnp.exp(-gate)) * (acc[1] * scale_in)).astype(bf16)
        elif kind == "dn":
            net.columns_down(rest[1])
            at = lax.rem(z // 2 + rest[1], NX)
            cut = SPLIT["d"]
            term = jnp.zeros((TOK, COLS), f32)
            for route, lanes in (("a", pl.ds(0, cut)), ("b", pl.ds(cut, FFT - cut))):
                rows_d = rows_of("d", route, 0, 2 * at) + rows_of("d", route, 0, 2 * at + 1)
                term = term + dot(hid[:, lanes], jnp.concatenate(rows_d, axis=0), ((1,), (1,)))
            part2[at] = term.astype(bf16)

            @pl.when(at != tp)
            def _():
                copy_to(
                    part2.at[at], rpart2.at[tp], ss.at[9], rs.at[9], {"sp": sp, "tp": at}
                ).start()
        else:
            getattr(net, kind)(*rest)
    total = resid_f + part2[tp].astype(f32)
    joint(9, rpart2.at[pl.ds(0, NX - 1)]).wait_recv()
    for r in range(1, NX):
        total = total + rpart2[xfrom[r]].astype(f32)
    o_ref[...] = total.astype(bf16)
    for n, ref in enumerate(
        (
            small1.at[pl.ds(0, NG - 1)],
            r1.at[pl.ds(0, NG - 1)],
            small2.at[pl.ds(0, NZ - 1)],
            r2.at[pl.ds(0, NZ - 1)],
            r3.at[pl.ds(0, NG - 1)],
            rsq.at[0, pl.ds(0, NX - 1)],
            rpart.at[pl.ds(0, NX - 1)],
            rsq.at[1, pl.ds(0, NX - 1)],
            y_ref.at[pl.ds(0, NX - 1)],
            rpart2.at[pl.ds(0, NX - 1)],
        )
    ):
        joint(n, ref).wait_send()
    net.drain()


def local(
    stream,
    queries,
    keys,
    values,
    out_gate,
    input_gate,
    forget_gate,
    head_gain,
    w_out,
    ffn_gain,
    w_gate,
    w_up,
    w_down,
):
    vmem = pl.BlockSpec(memory_space=pltpu.VMEM)
    hbm = pl.BlockSpec(memory_space=pl.ANY)
    return pl.pallas_call(
        layer_kernel,
        out_shape=jax.ShapeDtypeStruct((TOK, COLS), bf16),
        in_specs=[vmem] * 7 + [hbm] + [vmem] * 2 + [hbm] * 3,
        out_specs=vmem,
        scratch_shapes=[
            pltpu.VMEM((2, NZ, 2, 4, 32, SPLIT["u"]), bf16),
            pltpu.VMEM((2, NZ, 2, 4, 32, FFT - SPLIT["u"]), bf16),
            pltpu.VMEM((1, NZ, 2, 4, 32, SPLIT["d"]), bf16),
            pltpu.VMEM((1, NZ, 2, 4, 32, FFT - SPLIT["d"]), bf16),
            pltpu.VMEM((COLS, D), bf16),
            pltpu.VMEM((2, TOK, FFT), f32),
            pltpu.VMEM((TOK, FFT), bf16),
            pltpu.VMEM((NX, TOK, COLS), bf16),
            pltpu.VMEM((NG, 8, TOK), f32),
            pltpu.VMEM((NZ, 8, TOK), f32),
            pltpu.VMEM((NG, 8, TOK), f32),
            pltpu.VMEM((8, TOK), f32),
            pltpu.VMEM((8, TOK), f32),
            pltpu.VMEM((NG, 32, DV), bf16),
            pltpu.VMEM((NG, 32, DV), bf16),
            pltpu.VMEM((NG, 32, DV), f32),
            pltpu.VMEM((32, DV), bf16),
            pltpu.VMEM((NZ, 32, DV), bf16),
            pltpu.VMEM((NG, 32, DV), bf16),
            pltpu.VMEM((NG, 32, DV), bf16),
            pltpu.VMEM((NX, TOK, COLS), bf16),
            pltpu.VMEM((NX, TOK, COLS), bf16),
            pltpu.VMEM((2, 8, TOK), f32),
            pltpu.VMEM((2, NX, 8, TOK), f32),
            pltpu.VMEM((TOK, COLS), bf16),
            pltpu.VMEM((NX, TOK, COLS), bf16),
            pltpu.VMEM((NX, TOK, COLS), bf16),
            pltpu.SemaphoreType.DMA((7,)),
            pltpu.SemaphoreType.DMA((10,)),
            pltpu.SemaphoreType.DMA((10,)),
            pltpu.SemaphoreType.DMA((5 * RING,)),
            pltpu.SemaphoreType.DMA((76,)),
        ],
        compiler_params=pltpu.CompilerParams(
            collective_id=0, has_side_effects=True, vmem_limit_bytes=60 * 2**20
        ),
    )(
        queries,
        keys,
        values,
        out_gate,
        input_gate.T,
        forget_gate.T,
        head_gain.reshape(1, COLS),
        w_out,
        stream,
        ffn_gain.reshape(1, D),
        w_gate,
        w_up,
        w_down.T,
    )


def solution(mesh):
    in_specs = (
        P("sp", "tp"),
        P("sp", "tp"),
        P("sp", "tp"),
        P("sp", "tp"),
        P("sp", "tp"),
        P("sp", "tp"),
        P("sp", "tp"),
        P("tp"),
        P("tp", None),
        P(),
        P("sp", "tp"),
        P("sp", "tp"),
        P("tp", "sp"),
    )
    return jax.shard_map(
        local, mesh=mesh, in_specs=in_specs, out_specs=P("sp", "tp"), check_vma=False
    )
```

time: 83.9 us -> 77.5 us (0.924)
  the two profiles are of different devices: /device:TPU:5 before, /device:TPU:1 now
where the time goes in v4:
time: 77.5 us; the launch traced here: 76.7 us
  Pallas kernels  75.1 us (97%)
  local copies, waits for them, and re-layouts  1.57 us (2%)
    pallas_call x1, Pallas kernels, local(): pl.pallas_call(layer_kernel, out_shape=jax.ShapeDtypeStruct((TOK, COLS),...  75.1 us
    unnamed x1, local copies, waits for them, and re-layouts  1.57 us

profile of v4, /device:TPU:1, one launch (start us, length us, event | category | flops | bytes accessed | tf_op | source)
XLA Modules:
  0.0 76.7 jit_solution(15976252974160356097)
XLA Ops:
  0.0 75.1 %shard_map.127 = bf16[128,512]{1,0:T(8,128)(2,1)} custom-call(bf16[128,256]{1,0:T(8,128)(2,1)} %q_ref.1, bf16[128,256]{1,0:T(8,128)(2,1)} %k_ref.1, bf16[128,512]{1,0:T(8,128)(2,1)} %v_ref.1, bf16[128,512]{1,0:T(8,128)(2,1)} %og_ref.1, f32[2,128]{1,0:T(2,128)} %bitcast.8, f32[2,128]{1,0:T(2,128)} %bitcast.9, f32[1,512]{1,0:T(1,128)} %bitcast.7, ...), custom_call_target="tpu_custom_call" | custom-call | tf_op jit(solution)/shard_map/pallas_call | solution.py:669
  75.2 1.6 %copy.15 = bf16[128,512]{1,0:T(8,128)(2,1)} copy(bf16[128,512]{1,0:T(8,128)(2,1)} %shard_map.127) | data formatting | bytes 262144

commit v5 on v4

--- a/solution.py
+++ b/solution.py
@@ -60,130 +60,134 @@
 
 RING = 6
 COLUMNS = (0, -1, 1, -2, 2, -3, 3, 4)
-GROUPS = {0: (0, -1, 1), 1: (2, 3), 3: (-2, -3), 2: (4,)}
-GROUP_OF = {k: m for m, ks in GROUPS.items() for k in ks}
 SPLIT = {"u": 512, "d": 640}
 STEPS = {
     "first": (
-        ("own", "u"),
-        ("by", "u", 0),
+        ("own", "d"),
+    ),
+    "gates": (
     ),
     "slices": (
+        ("own", "u"),
+        ("by", "d", 0),
+        ("bz", "d", 1),
+        ("by", "d", 2),
+        ("by", "d", 1),
     ),
     "totals": (
         ("ayf", "u"),
+        ("byf", "d", 0),
+        ("ayf", "d"),
         ("bz", "u", 1),
-        ("by", "u", 1),
+        ("by", "u", 0),
         ("by", "u", 2),
-        ("byf", "u", 0),
+        ("byf", "d", 1),
         ("az", "u", 0),
-        ("sa", "u", 0),
-        ("byf", "u", 1),
+        ("bz", "u", 2),
     ),
     "prefix": (
-        ("own", "d"),
-        ("bz", "u", 2),
+        ("bz", "d", 2),
+        ("by", "u", 4),
         ("by", "u", 3),
-        ("by", "u", 4),
-        ("byf", "u", 2),
-        ("sb", "u", 0),
-        ("sb", "u", 1),
+        ("by", "u", 1),
+        ("az", "u", 1),
+        ("az", "d", 0),
     ),
     "parts": (
-        ("az", "u", 1),
-        ("sa", "u", -1),
-        ("sa", "u", 1),
-        ("ayf", "d"),
-        ("byf", "u", 3),
-        ("bz", "d", 1),
+        ("sb", "d", 0),
         ("bz", "u", 3),
         ("by", "u", 5),
-        ("by", "u", 6),
+        ("sb", "d", 1),
+        ("byf", "u", 3),
+        ("sa", "u", 0),
         ("byf", "u", 4),
-        ("sb", "u", 2),
-        ("az", "d", 0),
         ("sa", "d", 0),
-        ("sb", "u", 3),
-        ("az", "u", 2),
-        ("sa", "u", -2),
+        ("byf", "u", 1),
+        ("sa", "u", 1),
     ),
     "feats": (
+        ("az", "u", 2),
+        ("byf", "u", 0),
+        ("byf", "u", 2),
         ("sa", "u", 2),
-        ("by", "d", 0),
+        ("sb", "u", 3),
         ("byf", "u", 5),
+        ("sa", "u", -1),
+        ("az", "d", 1),
+        ("sb", "u", 4),
+        ("by", "u", 6),
+        ("sb", "u", 1),
         ("bz", "u", 4),
+        ("sb", "u", 2),
+        ("byf", "d", 2),
         ("by", "u", 7),
-        ("byf", "u", 6),
-        ("sb", "u", 4),
-        ("bz", "d", 2),
-        ("az", "d", 1),
+        ("by", "d", 4),
+        ("sb", "u", 0),
+        ("sb", "u", 5),
         ("sa", "d", -1),
-        ("sa", "d", 1),
-        ("by", "d", 1),
-        ("sb", "u", 5),
+        ("sb", "d", 2),
+        ("az", "u", 3),
     ),
     "rest": (
-        ("fa", "u", -2),
+        ("byf", "u", 6),
+        ("fb", "u", 2),
         ("fa", "u", -1),
-        ("fb", "u", 0),
-        ("fa", "u", 0),
-        ("fb", "u", 1),
-        ("fa", "u", 1),
-        ("fb", "u", 2),
-        ("fa", "u", 2),
+        ("sa", "u", -3),
         ("fb", "u", 3),
         ("byf", "u", 7),
+        ("bz", "d", 3),
+        ("by", "d", 6),
+        ("fa", "u", 1),
+        ("fb", "u", 5),
+        ("sa", "u", 3),
+        ("by", "d", 3),
+        ("sa", "u", -2),
+        ("fa", "u", 3),
+        ("az", "d", 2),
+        ("sb", "u", 6),
+        ("fb", "u", 0),
+        ("by", "d", 5),
+        ("sb", "u", 7),
+        ("fa", "u", 2),
         ("fb", "u", 4),
-        ("fb", "u", 5),
-        ("by", "d", 2),
-        ("by", "d", 3),
-        ("sb", "u", 6),
-        ("by", "d", 4),
-        ("az", "u", 3),
-        ("sa", "u", -3),
-        ("sa", "u", 3),
-        ("byf", "d", 0),
-        ("byf", "d", 1),
-        ("bz", "d", 3),
         ("fb", "u", 6),
-        ("sb", "u", 7),
-        ("by", "d", 5),
-        ("fa", "u", -3),
-        ("by", "d", 6),
-        ("fa", "u", 3),
-        ("byf", "d", 2),
-        ("fb", "u", 7),
-        ("az", "d", 2),
-        ("byf", "d", 3),
-        ("sa", "d", -2),
-        ("sa", "d", 2),
         ("byf", "d", 4),
-        ("sb", "d", 0),
-        ("sb", "d", 1),
-        ("byf", "d", 5),
         ("az", "u", 4),
         ("sa", "u", 4),
+        ("sa", "d", 1),
+        ("sa", "d", -2),
         ("bz", "d", 4),
+        ("fa", "u", 0),
         ("by", "d", 7),
+        ("fb", "u", 1),
+        ("sa", "d", 2),
+        ("fa", "u", -2),
+        ("fb", "u", 7),
+        ("byf", "d", 3),
+        ("fa", "u", 4),
+        ("fa", "u", -3),
+        ("byf", "d", 5),
+        ("hid", "u"),
         ("byf", "d", 6),
-        ("sb", "d", 2),
+        ("dn", "d", -1),
+        ("sb", "d", 4),
+        ("dn", "d", 1),
+        ("az", "d", 3),
+        ("byf", "d", 7),
+        ("sa", "d", -3),
+        ("dn", "d", 2),
         ("sb", "d", 3),
-        ("fa", "u", 4),
-        ("hid", "u"),
-        ("sb", "d", 4),
+        ("sa", "d", 3),
+        ("sb", "d", 5),
         ("dn", "d", 0),
-        ("sb", "d", 5),
-        ("byf", "d", 7),
-        ("az", "d", 3),
-        ("sa", "d", -3),
-        ("sa", "d", 3),
         ("sb", "d", 6),
-        ("dn", "d", 3),
+        ("dn", "d", -2),
         ("sb", "d", 7),
-        ("dn", "d", 1),
+        ("dn", "d", -3),
         ("az", "d", 4),
         ("sa", "d", 4),
-        ("dn", "d", 2),
+        ("dn", "d", 3),
+        ("dn", "d", 4),
     ),
 }
 
@@ -268,8 +272,7 @@
 
     def sb(self, f, j):
         self.got(f"byf{f}{j}", self.at(f, "b", self.zi[j], self.yk(2)))
-        group = j if f == "u" else GROUP_OF[COLUMNS[j]]
-        self.send(f"sb{f}{group}", "s", self.at(f, "b", self.zi[j], pl.ds(0, 4)))
+        self.send(f"sb{f}{j}", "s", self.at(f, "b", self.zi[j], pl.ds(0, 4)))
 
     def ayf(self, f):
         self.got(f"ay{f}", self.at(f, "a", self.z, pl.ds(0, 2)))
@@ -277,8 +280,7 @@
         self.send(f"ayf{f}", "y-", self.at(f, "a", self.z, self.yk(1), 1))
 
     def sa(self, f, k):
-        group = k if f == "u" else GROUP_OF[k]
-        self.send(f"sa{f}{group}", "s", self.at(f, "a", self.zk(k), pl.ds(0, 4)))
+        self.send(f"sa{f}{k}", "s", self.at(f, "a", self.zk(k), pl.ds(0, 4)))
 
     def az(self, f, k):
         if k == 0:
@@ -292,15 +294,11 @@
                 if k < 3 or p == mine:
                     self.send(f"az{f}{k + 1}", way, self.at(f, "a", zi, pl.ds(2 * p, 2)))
 
-    def column_b(self, j):
-        self.got(f"sbu{j}", self.at("u", "b", self.zi[j], pl.ds(0, 4)))
-
-    def column_a(self, k):
-        self.got(f"sau{k}", self.at("u", "a", self.zk(k), pl.ds(0, 4)))
-
-    def columns_down(self, m):
-        for route in "ab":
-            self.got(f"s{route}d{m}", self.at("d", route, pl.ds(0, len(GROUPS[m])), pl.ds(0, 4)))
+    def column_b(self, f, j):
+        self.got(f"sb{f}{j}", self.at(f, "b", self.zi[j], pl.ds(0, 4)))
+
+    def column_a(self, f, k):
+        self.got(f"sa{f}{k}", self.at(f, "a", self.zk(k), pl.ds(0, 4)))
 
     def slot(self, name):
         for kind, *rest in STEPS[name]:
@@ -308,16 +306,16 @@
 
 
 def layer_kernel(
-    q_ref,
-    k_ref,
-    v_ref,
-    og_ref,
-    ig_ref,
-    fg_ref,
-    hg_ref,
+    q_hbm,
+    k_hbm,
+    v_hbm,
+    og_hbm,
+    ig_hbm,
+    fg_hbm,
+    hg_hbm,
     wo_hbm,
-    st_ref,
-    gain_ref,
+    st_hbm,
+    gain_hbm,
     wg_hbm,
     wu_hbm,
     wd_hbm,
@@ -326,7 +324,16 @@
     ub,
     da,
     db,
+    q_ref,
+    k_ref,
+    v_ref,
+    og_ref,
+    ig_ref,
+    fg_ref,
+    hg_ref,
     wo,
+    st_ref,
+    gain_ref,
     acc,
     hid,
     y_ref,
@@ -380,9 +387,18 @@
                     ref.at[:, lanes], bufs[f, route].at[kind, z, net.c, net.y], lsem.at[len(loads)]
                 )
             )
-    loads.append(pltpu.make_async_copy(wo_hbm, wo, lsem.at[6]))
+    early = ((fg_hbm, fg_ref), (ig_hbm, ig_ref), (k_hbm, k_ref), (v_hbm, v_ref), (q_hbm, q_ref))
+    late = ((wo_hbm, wo), (og_hbm, og_ref), (hg_hbm, hg_ref), (st_hbm, st_ref), (gain_hbm, gain_ref))
+    for src, dst in early + late:
+        loads.append(pltpu.make_async_copy(src, dst, lsem.at[len(loads)]))
     for c in loads:
         c.start()
+    for c in loads[:6]:
+        c.wait()
+    pl.semaphore_wait(bar, count)
+    net.slot("first")
+    for c in loads[6:11]:
+        c.wait()
     rows = lax.broadcasted_iota(jnp.int32, (TOK, TOK), 0)
     cols = lax.broadcasted_iota(jnp.int32, (TOK, TOK), 1)
     eye = rows == cols
@@ -429,13 +445,10 @@
         den0.append(jnp.sum(scores, axis=1, keepdims=True))
         peak0.append(peak)
 
-    pl.semaphore_wait(bar, count)
+    net.slot("gates")
     for r in range(1, NG):
         copy_to(small_me, small1.at[g], ss.at[0], rs.at[0], gdev[r]).start()
         copy_to(s_loc.at[gpeer[r]], r1.at[g], ss.at[1], rs.at[1], gdev[r]).start()
-    for c in loads[:6]:
-        c.wait()
-    net.slot("first")
     small1[g] = small_me[...]
     r1[g] = s_loc[g]
     net.slot("slices")
@@ -528,6 +541,8 @@
         copy_to(o3.at[gpeer[r]], r3.at[g], ss.at[4], rs.at[4], gdev[r]).start()
     r3[g] = o3[g]
     net.slot("prefix")
+    for c in loads[11:]:
+        c.wait()
     gates = [
         hg_ref[:, h * DV : (h + 1) * DV]
         / (1.0 + jnp.exp(-og_ref[:, h * DV : (h + 1) * DV].astype(f32)))
@@ -546,7 +561,6 @@
         copy_to(sq_me.at[0], rsq.at[0, tp], ss.at[5], rs.at[5], xdev[r]).start()
     rsq[0, tp] = sq_me[0]
     heads = jnp.concatenate(gated, axis=1)
-    loads[6].wait()
     for r in (2, 1, 3, 0):
         at = pl.multiple_of(xpeer[r] * COLS, COLS)
         part[xpeer[r]] = dot(heads, wo[:, pl.ds(at, COLS)]).astype(bf16)
@@ -601,36 +615,44 @@
 
     for kind, *rest in STEPS["rest"]:
         if kind == "fb":
-            net.column_b(rest[1])
+            net.column_b(*rest)
             column("b", net.zi[rest[1]])
         elif kind == "fa":
-            net.column_a(rest[1])
+            net.column_a(*rest)
             column("a", net.zk(rest[1]))
         elif kind == "hid":
             gate = acc[0] * scale_in
             hid[...] = (gate / (1.0 + jnp.exp(-gate)) * (acc[1] * scale_in)).astype(bf16)
         elif kind == "dn":
-            net.columns_down(rest[1])
-            at = lax.rem(z // 2 + rest[1], NX)
+            net.column_b("d", COLUMNS.index(rest[1]))
+            net.column_a("d", rest[1])
+            zi = net.zk(rest[1])
+            at = zi // 2
             cut = SPLIT["d"]
-            term = jnp.zeros((TOK, COLS), f32)
+            term = jnp.zeros((TOK, 256), f32)
             for route, lanes in (("a", pl.ds(0, cut)), ("b", pl.ds(cut, FFT - cut))):
-                rows_d = rows_of("d", route, 0, 2 * at) + rows_of("d", route, 0, 2 * at + 1)
-                term = term + dot(hid[:, lanes], jnp.concatenate(rows_d, axis=0), ((1,), (1,)))
-            part2[at] = term.astype(bf16)
+                rows_d = jnp.concatenate(rows_of("d", route, 0, zi), axis=0)
+                term = term + dot(hid[:, lanes], rows_d, ((1,), (1,)))
+            part2[zi] = term.astype(bf16)
 
             @pl.when(at != tp)
             def _():
                 copy_to(
-                    part2.at[at], rpart2.at[tp], ss.at[9], rs.at[9], {"sp": sp, "tp": at}
+                    part2.at[zi],
+                    rpart2.at[tp, lax.rem(zi, 2)],
+                    ss.at[9],
+                    rs.at[9],
+                    {"sp": sp, "tp": at},
                 ).start()
         else:
             getattr(net, kind)(*rest)
-    total = resid_f + part2[tp].astype(f32)
     joint(9, rpart2.at[pl.ds(0, NX - 1)]).wait_recv()
-    for r in range(1, NX):
-        total = total + rpart2[xfrom[r]].astype(f32)
-    o_ref[...] = total.astype(bf16)
+    for half in range(2):
+        lanes = slice(256 * half, 256 * half + 256)
+        total = resid_f[:, lanes] + part2[2 * tp + half].astype(f32)
+        for r in range(1, NX):
+            total = total + rpart2[xfrom[r], half].astype(f32)
+        o_ref[:, lanes] = total.astype(bf16)
     for n, ref in enumerate(
         (
             small1.at[pl.ds(0, NG - 1)],
@@ -668,15 +690,24 @@
     hbm = pl.BlockSpec(memory_space=pl.ANY)
     return pl.pallas_call(
         layer_kernel,
-        out_shape=jax.ShapeDtypeStruct((TOK, COLS), bf16),
-        in_specs=[vmem] * 7 + [hbm] + [vmem] * 2 + [hbm] * 3,
+        out_shape=pltpu.VMEM((TOK, COLS), bf16),
+        in_specs=[hbm] * 13,
         out_specs=vmem,
         scratch_shapes=[
             pltpu.VMEM((2, NZ, 2, 4, 32, SPLIT["u"]), bf16),
             pltpu.VMEM((2, NZ, 2, 4, 32, FFT - SPLIT["u"]), bf16),
             pltpu.VMEM((1, NZ, 2, 4, 32, SPLIT["d"]), bf16),
             pltpu.VMEM((1, NZ, 2, 4, 32, FFT - SPLIT["d"]), bf16),
+            pltpu.VMEM((TOK, 2 * DQK), bf16),
+            pltpu.VMEM((TOK, 2 * DQK), bf16),
+            pltpu.VMEM((TOK, COLS), bf16),
+            pltpu.VMEM((TOK, COLS), bf16),
+            pltpu.VMEM((2, TOK), f32),
+            pltpu.VMEM((2, TOK), f32),
+            pltpu.VMEM((1, COLS), f32),
             pltpu.VMEM((COLS, D), bf16),
+            pltpu.VMEM((TOK, COLS), bf16),
+            pltpu.VMEM((1, D), f32),
             pltpu.VMEM((2, TOK, FFT), f32),
             pltpu.VMEM((TOK, FFT), bf16),
             pltpu.VMEM((NX, TOK, COLS), bf16),
@@ -697,13 +728,13 @@
             pltpu.VMEM((2, 8, TOK), f32),
             pltpu.VMEM((2, NX, 8, TOK), f32),
             pltpu.VMEM((TOK, COLS), bf16),
-            pltpu.VMEM((NX, TOK, COLS), bf16),
-            pltpu.VMEM((NX, TOK, COLS), bf16),
-            pltpu.SemaphoreType.DMA((7,)),
+            pltpu.VMEM((NZ, TOK, 256), bf16),
+            pltpu.VMEM((NX, 2, TOK, 256), bf16),
+            pltpu.SemaphoreType.DMA((16,)),
             pltpu.SemaphoreType.DMA((10,)),
             pltpu.SemaphoreType.DMA((10,)),
             pltpu.SemaphoreType.DMA((5 * RING,)),
-            pltpu.SemaphoreType.DMA((76,)),
+            pltpu.SemaphoreType.DMA((84,)),
         ],
         compiler_params=pltpu.CompilerParams(
             collective_id=0, has_side_effects=True, vmem_limit_bytes=60 * 2**20

time: 77.5 us -> 71.6 us (0.924)
  Pallas kernels: 75.1 us -> 69.7 us
  local copies, waits for them, and re-layouts: 1.57 us -> 0.66 us
    pallas_call x1, Pallas kernels: 75.1 us -> 69.7 us  [local(): pl.pallas_call(layer_kernel, out_shape=pltpu.VMEM((TOK, COLS), bf16), in_...]
    unnamed x1, local copies, waits for them, and re-layouts: 1.57 us -> 0.66 us
where the time goes in v5:
time: 71.6 us; the launch traced here: 70.4 us
  Pallas kernels  69.7 us (97%)
    pallas_call x1, Pallas kernels, local(): pl.pallas_call(layer_kernel, out_shape=pltpu.VMEM((TOK, COLS), bf16), in_...  69.7 us

profile of v5, /device:TPU:1, one launch (start us, length us, event | category | flops | bytes accessed | tf_op | source)
XLA Modules:
  0.0 70.4 jit_solution(10154633555566513769)
XLA Ops:
  0.0 69.7 %shard_map.127 = bf16[128,512]{1,0:T(8,128)(2,1)S(1)} custom-call(bf16[128,256]{1,0:T(8,128)(2,1)} %q_hbm.1, bf16[128,256]{1,0:T(8,128)(2,1)} %k_hbm.1, bf16[128,512]{1,0:T(8,128)(2,1)} %v_hbm.1, bf16[128,512]{1,0:T(8,128)(2,1)} %og_hbm.1, f32[2,128]{1,0:T(2,128)} %bitcast.8, f32[2,128]{1,0:T(2,128)} %bitcast.9, f32[1,512]{1,0:T(1,128)} %bitcast.7, ...), custom_call_target="tpu_custom_call" | custom-call | tf_op jit(solution)/shard_map/pallas_call | solution.py:691
  69.8 0.7 copy.15

commit v6 on v5

--- a/solution.py
+++ b/solution.py
@@ -69,121 +69,121 @@
     ),
     "slices": (
         ("own", "u"),
+        ("by", "u", 0),
+        ("bz", "d", 1),
         ("by", "d", 0),
-        ("bz", "d", 1),
-        ("by", "d", 2),
-        ("by", "d", 1),
     ),
     "totals": (
         ("ayf", "u"),
-        ("byf", "d", 0),
-        ("ayf", "d"),
         ("bz", "u", 1),
-        ("by", "u", 0),
         ("by", "u", 2),
-        ("byf", "d", 1),
         ("az", "u", 0),
-        ("bz", "u", 2),
+        ("by", "u", 1),
+        ("by", "d", 1),
     ),
     "prefix": (
+        ("bz", "u", 2),
+        ("byf", "u", 0),
+        ("sa", "u", 0),
+        ("by", "u", 3),
+        ("by", "d", 2),
         ("bz", "d", 2),
-        ("by", "u", 4),
-        ("by", "u", 3),
-        ("by", "u", 1),
+        ("byf", "u", 1),
+        ("ayf", "d"),
         ("az", "u", 1),
-        ("az", "d", 0),
+        ("bz", "u", 3),
+        ("by", "u", 5),
     ),
     "parts": (
-        ("sb", "d", 0),
-        ("bz", "u", 3),
-        ("by", "u", 5),
-        ("sb", "d", 1),
+        ("byf", "u", 2),
         ("byf", "u", 3),
-        ("sa", "u", 0),
-        ("byf", "u", 4),
-        ("sa", "d", 0),
-        ("byf", "u", 1),
-        ("sa", "u", 1),
-    ),
-    "feats": (
-        ("az", "u", 2),
-        ("byf", "u", 0),
-        ("byf", "u", 2),
-        ("sa", "u", 2),
-        ("sb", "u", 3),
-        ("byf", "u", 5),
-        ("sa", "u", -1),
-        ("az", "d", 1),
-        ("sb", "u", 4),
+        ("by", "u", 4),
+        ("az", "d", 0),
         ("by", "u", 6),
         ("sb", "u", 1),
         ("bz", "u", 4),
+        ("az", "u", 2),
         ("sb", "u", 2),
+        ("sb", "u", 0),
+        ("sa", "u", -1),
+        ("by", "u", 7),
+        ("sa", "d", 0),
+    ),
+    "feats": (
+        ("sa", "u", 2),
+        ("sa", "u", -2),
+        ("sa", "u", 1),
+        ("byf", "u", 5),
+        ("byf", "u", 4),
+        ("byf", "d", 0),
+        ("byf", "u", 6),
+        ("sb", "u", 3),
+        ("az", "d", 1),
+        ("byf", "u", 7),
+        ("sb", "u", 5),
+        ("az", "u", 3),
+        ("byf", "d", 1),
         ("byf", "d", 2),
-        ("by", "u", 7),
-        ("by", "d", 4),
-        ("sb", "u", 0),
-        ("sb", "u", 5),
-        ("sa", "d", -1),
-        ("sb", "d", 2),
-        ("az", "u", 3),
+        ("sb", "u", 4),
+        ("bz", "d", 3),
+        ("sb", "d", 0),
     ),
     "rest": (
-        ("byf", "u", 6),
+        ("by", "d", 4),
+        ("sa", "d", -1),
         ("fb", "u", 2),
-        ("fa", "u", -1),
+        ("fb", "u", 1),
+        ("fb", "u", 0),
+        ("by", "d", 3),
         ("sa", "u", -3),
-        ("fb", "u", 3),
-        ("byf", "u", 7),
-        ("bz", "d", 3),
-        ("by", "d", 6),
         ("fa", "u", 1),
         ("fb", "u", 5),
-        ("sa", "u", 3),
-        ("by", "d", 3),
-        ("sa", "u", -2),
-        ("fa", "u", 3),
+        ("by", "d", 5),
+        ("sb", "u", 7),
         ("az", "d", 2),
         ("sb", "u", 6),
-        ("fb", "u", 0),
-        ("by", "d", 5),
-        ("sb", "u", 7),
+        ("sa", "u", 3),
+        ("by", "d", 6),
+        ("fb", "u", 4),
+        ("fa", "u", -2),
         ("fa", "u", 2),
-        ("fb", "u", 4),
-        ("fb", "u", 6),
-        ("byf", "d", 4),
         ("az", "u", 4),
         ("sa", "u", 4),
+        ("byf", "d", 4),
+        ("fa", "u", -3),
+        ("byf", "d", 3),
+        ("fb", "u", 7),
+        ("bz", "d", 4),
+        ("by", "d", 7),
+        ("sb", "d", 1),
+        ("fb", "u", 6),
+        ("sa", "d", -2),
+        ("fa", "u", -1),
+        ("fa", "u", 3),
+        ("sb", "d", 2),
+        ("fa", "u", 0),
+        ("sa", "d", 2),
+        ("fb", "u", 3),
         ("sa", "d", 1),
-        ("sa", "d", -2),
-        ("bz", "d", 4),
-        ("fa", "u", 0),
-        ("by", "d", 7),
-        ("fb", "u", 1),
-        ("sa", "d", 2),
-        ("fa", "u", -2),
-        ("fb", "u", 7),
-        ("byf", "d", 3),
         ("fa", "u", 4),
-        ("fa", "u", -3),
         ("byf", "d", 5),
         ("hid", "u"),
+        ("dn", "d", 0),
+        ("dn", "d", -1),
         ("byf", "d", 6),
-        ("dn", "d", -1),
+        ("sb", "d", 3),
         ("sb", "d", 4),
+        ("az", "d", 3),
+        ("sa", "d", -3),
+        ("byf", "d", 7),
         ("dn", "d", 1),
-        ("az", "d", 3),
-        ("byf", "d", 7),
-        ("sa", "d", -3),
+        ("sb", "d", 5),
+        ("dn", "d", -2),
+        ("sb", "d", 6),
+        ("sa", "d", 3),
         ("dn", "d", 2),
-        ("sb", "d", 3),
-        ("sa", "d", 3),
-        ("sb", "d", 5),
-        ("dn", "d", 0),
-        ("sb", "d", 6),
-        ("dn", "d", -2),
+        ("dn", "d", -3),
         ("sb", "d", 7),
-        ("dn", "d", -3),
         ("az", "d", 4),
         ("sa", "d", 4),
         ("dn", "d", 3),
@@ -375,6 +375,7 @@
     def joint(n, ref):
         return copy_to(ref, ref, ss.at[n], rs.at[n], gdev[1])
 
+    r2[...] = jnp.zeros_like(r2)
     bar, count = barrier_all(gdev[1:] + zdev[1:] + xdev[1:])
     bufs = {("u", "a"): ua, ("u", "b"): ub, ("d", "a"): da, ("d", "b"): db}
     net = Weights(bufs, wss, wrs, z, g, tp)
@@ -395,8 +396,6 @@
         c.start()
     for c in loads[:6]:
         c.wait()
-    pl.semaphore_wait(bar, count)
-    net.slot("first")
     for c in loads[6:11]:
         c.wait()
     rows = lax.broadcasted_iota(jnp.int32, (TOK, TOK), 0)
@@ -445,6 +444,8 @@
         den0.append(jnp.sum(scores, axis=1, keepdims=True))
         peak0.append(peak)
 
+    pl.semaphore_wait(bar, count)
+    net.slot("first")
     net.slot("gates")
     for r in range(1, NG):
         copy_to(small_me, small1.at[g], ss.at[0], rs.at[0], gdev[r]).start()
@@ -492,7 +493,11 @@
         run = spread(mine(f_list[i])) * run + spread(mine(l_list[i])) * r1[i].astype(f32)
     t_loc[...] = run.astype(bf16)
     for r in range(1, NZ):
-        copy_to(t_loc, r2.at[z], ss.at[3], rs.at[3], zdev[r]).start()
+
+        @pl.when(z + r < NZ)
+        def _(r=r):
+            copy_to(t_loc, r2.at[z], ss.at[10 + r], rs.at[10 + r], zdev[r]).start()
+
     r2[z] = t_loc[...]
     net.slot("totals")
 
@@ -531,7 +536,12 @@
         scale0.append(s0 * inv)
         carried.append(c0 * inv)
 
-    joint(3, r2.at[pl.ds(0, NZ - 1)]).wait_recv()
+    for r in range(1, NZ):
+
+        @pl.when(z >= r)
+        def _(r=r):
+            joint(10 + r, r2.at[0]).wait_recv()
+
     run = jnp.zeros((32, DV), f32)
     for i in range(NZ):
         run = spread(fz[i]) * run + spread(lz[i]) * r2[i].astype(f32)
@@ -658,7 +668,7 @@
             small1.at[pl.ds(0, NG - 1)],
             r1.at[pl.ds(0, NG - 1)],
             small2.at[pl.ds(0, NZ - 1)],
-            r2.at[pl.ds(0, NZ - 1)],
+            None,
             r3.at[pl.ds(0, NG - 1)],
             rsq.at[0, pl.ds(0, NX - 1)],
             rpart.at[pl.ds(0, NX - 1)],
@@ -667,7 +677,14 @@
             rpart2.at[pl.ds(0, NX - 1)],
         )
     ):
-        joint(n, ref).wait_send()
+        if ref is not None:
+            joint(n, ref).wait_send()
+    for r in range(1, NZ):
+
+        @pl.when(z + r < NZ)
+        def _(r=r):
+            joint(10 + r, r2.at[0]).wait_send()
+
     net.drain()
 
 
@@ -731,8 +748,8 @@
             pltpu.VMEM((NZ, TOK, 256), bf16),
             pltpu.VMEM((NX, 2, TOK, 256), bf16),
             pltpu.SemaphoreType.DMA((16,)),
-            pltpu.SemaphoreType.DMA((10,)),
-            pltpu.SemaphoreType.DMA((10,)),
+            pltpu.SemaphoreType.DMA((18,)),
+            pltpu.SemaphoreType.DMA((18,)),
             pltpu.SemaphoreType.DMA((5 * RING,)),
             pltpu.SemaphoreType.DMA((84,)),
         ],

time: 71.6 us -> 71.4 us (level)
  the two profiles are of different devices: /device:TPU:1 before, /device:TPU:37 now
where the time goes in v6:
time: 71.4 us; the launch traced here: 71.3 us
  Pallas kernels  70.6 us (99%)
    pallas_call x1, Pallas kernels, local(): pl.pallas_call(layer_kernel, out_shape=pltpu.VMEM((TOK, COLS), bf16), in_...  70.6 us

profile of v6, /device:TPU:37, one launch (start us, length us, event | category | flops | bytes accessed | tf_op | source)
XLA Modules:
  0.0 71.3 jit_solution(513907712895501865)
XLA Ops:
  0.0 70.6 %shard_map.127 = bf16[128,512]{1,0:T(8,128)(2,1)S(1)} custom-call(bf16[128,256]{1,0:T(8,128)(2,1)} %q_hbm.1, bf16[128,256]{1,0:T(8,128)(2,1)} %k_hbm.1, bf16[128,512]{1,0:T(8,128)(2,1)} %v_hbm.1, bf16[128,512]{1,0:T(8,128)(2,1)} %og_hbm.1, f32[2,128]{1,0:T(2,128)} %bitcast.8, f32[2,128]{1,0:T(2,128)} %bitcast.9, f32[1,512]{1,0:T(1,128)} %bitcast.7, ...), custom_call_target="tpu_custom_call" | custom-call | tf_op jit(solution)/shard_map/pallas_call | solution.py:708
  70.7 0.7 copy.15
